TPU v7x, 32 devices: a whole 2x2x4 slice. The times are simulated.
32 devices in a mesh: sp: 16 (over z, y, core), tp: 2 (over x).
Axes of the slice: x: 2, y: 2, z: 4, core: 2. Of those that a mesh axis runs over, the one named last changes fastest.
Arguments:
- inputs: bfloat16 [4096, 4096], P('sp', 'tp'), may hold values from -20 to 20
- norm_gain: float32 [3, 4096], replicated, may hold values from 0.1 to 1.9
- in_weight: bfloat16 [3, 4096, 1024], P(None, 'tp', 'sp'), may hold values from -0.09375 to 0.09375
- pool_scale: float32 [3, 1024], replicated, may hold values from 0.1 to 1.9
- out_weight: bfloat16 [3, 1024, 4096], P(None, 'sp', 'tp'), may hold values from -0.1875 to 0.1875
Outputs:
- final_state: bfloat16 [4096, 4096], P('sp', 'tp')
All inputs are finite; a program needn't handle non-finite values.
Results may differ from a plain program's by a relative error of at most 0.017.
Values may be sent and summed in bfloat16 or wider, within the bound.
A program may use at most 64 MiB of HBM per device.

v0:
```python
import functools

import jax
import jax.numpy as jnp
from jax import lax
from jax.experimental import pallas as pl
from jax.experimental.pallas import tpu as pltpu
from jax.sharding import PartitionSpec as P

EPS = 1e-06
REACH = 16
GROUPS = 4
MESH_ID = pl.DeviceIdType.MESH


def shift_sp(value):
    count = lax.axis_size("sp")
    return lax.ppermute(value, "sp", [(i, i + 1) for i in range(count - 1)])


def window_means(extended, row_count, first_channel, first_pos, pool_total):
    width = extended.shape[1]
    channel = first_channel + lax.broadcasted_iota(jnp.int32, (1, width), 1)
    window_len = jnp.left_shift(jnp.int32(2), channel // (pool_total // GROUPS))
    running = jnp.zeros((row_count, width), jnp.float32)
    for offset in range(REACH):
        shifted = extended[REACH - offset : REACH - offset + row_count]
        running = running + jnp.where(offset < window_len, shifted, 0.0)
    position = first_pos + lax.broadcasted_iota(jnp.int32, (row_count, 1), 0)
    divisor = jnp.minimum(position + 1, window_len).astype(jnp.float32)
    return running / divisor - extended[REACH:]


def plain_body(inputs, norm_gain, in_weight, pool_scale, out_weight):
    rows, feats = inputs.shape
    layers, features = norm_gain.shape
    pools = pool_scale.shape[1]
    part = pools // lax.axis_size("tp")
    t = lax.axis_index("tp")
    s = lax.axis_index("sp")
    current = inputs
    for layer in range(layers):
        in_all = lax.all_gather(in_weight[layer], "sp", axis=1, tiled=True)
        out_all = lax.all_gather(out_weight[layer], "sp", axis=0, tiled=True)
        wide = current.astype(jnp.float32)
        squares = lax.psum(jnp.sum(wide * wide, axis=1), "tp")
        inv_rms = lax.rsqrt(squares / features + EPS)[:, None]
        gain = lax.dynamic_slice_in_dim(norm_gain[layer], t * feats, feats)
        normed = (wide * inv_rms * gain).astype(jnp.bfloat16)
        partial = jnp.dot(normed, in_all, preferred_element_type=jnp.float32)
        pool_in = lax.psum_scatter(
            partial.astype(jnp.bfloat16), "tp", scatter_dimension=1, tiled=True
        )
        edge = shift_sp(pool_in[rows - REACH :])
        extended = jnp.concatenate([edge, pool_in], 0).astype(jnp.float32)
        means = window_means(extended, rows, t * part, s * rows, pools)
        scale = lax.dynamic_slice_in_dim(pool_scale[layer], t * part, part)
        mixed = (means * scale).astype(jnp.bfloat16)
        pooled = lax.all_gather(mixed, "tp", axis=1, tiled=True)
        branch = jnp.dot(pooled, out_all, preferred_element_type=jnp.float32)
        current = (current.astype(jnp.float32) + branch).astype(jnp.bfloat16)
    return current


def kernel(
    n_z, layers, halo,
    x_ref, gain_ref, wi_ref, scale_ref, wo_ref, o_ref,
    held, state, xg, edge, p_own, p_send, p_recv, mix, sq_send, sq_recv,
    w_send, w_recv, local_sem, a_send, a_recv,
):
    rows, feats = x_ref.shape
    total = rows + halo
    blocks = held.shape[1]
    half = mix.shape[2] * mix.shape[4]
    pools = 2 * half
    phases = 2 * layers
    s = lax.axis_index("sp")
    t = lax.axis_index("tp")
    core = s % 2
    y = (s // 2) % 2
    z = s // 4

    def block_of(zz, yy, cc):
        return zz * 4 + yy * 2 + cc

    upper = z // 2
    near = z + 1 - 2 * (z % 2)
    across = n_z // 2 - upper
    far = (n_z - 1) * (1 - upper)
    at_end = jnp.logical_or(z == 0, z == n_z - 1)
    inside = jnp.logical_not(at_end)
    up, down = (z + 1) % n_z, (z + n_z - 1) % n_z
    has_up, has_down = z < n_z - 1, z > 0
    inner = jnp.where(upper == 0, up, down)
    outer = jnp.where(upper == 0, down, up)

    y_mate = (block_of(z, 1 - y, core), t)
    c_mate = (block_of(z, y, 1 - core), t)
    x_mate = (s, 1 - t)
    after = ((s + 1) % blocks, t)
    before = ((s + blocks - 1) % blocks, t)

    def along(zz):
        return (block_of(zz, y, core), t)

    barrier = pltpu.get_barrier_semaphore()
    peers = [along(up), along(down), y_mate, c_mate, x_mate, after, before]
    for peer in peers:
        pl.semaphore_signal(barrier, inc=1, device_id=peer, device_id_type=MESH_ID)
    pl.semaphore_wait(barrier, len(peers))

    sent = []

    def send(src, dst, send_sem, recv_sem, to, when=None):
        copy = pltpu.make_async_remote_copy(
            src_ref=src, dst_ref=dst, send_sem=send_sem, recv_sem=recv_sem,
            device_id=to, device_id_type=MESH_ID,
        )
        if when is None:
            copy.start()
        else:
            pl.when(when)(copy.start)
        sent.append((copy, when))

    def arrived(ref, sem):
        pltpu.make_async_remote_copy(
            src_ref=ref, dst_ref=ref, send_sem=sem, recv_sem=sem,
            device_id=c_mate, device_id_type=MESH_ID,
        ).wait_recv()

    depth = held.shape[2]
    whole, first, second = pl.ds(0, depth), pl.ds(0, depth // 2), pl.ds(depth // 2, depth // 2)

    def own(p):
        return (wi_ref if p % 2 == 0 else wo_ref).at[p // 2]

    count = [0] * phases

    def send_own(p, to, when=None):
        send(own(p), held.at[p, s], w_send.at[p, count[p]], w_recv.at[p, s, 0], to, when)
        count[p] += 1

    def forward(p, block, to, piece=None, when=None):
        piece = whole if piece is None else piece
        ref = held.at[p, block, piece]
        sem = w_recv.at[p, block, 1 if piece is second else 0]
        send(ref, ref, w_send.at[p, count[p]], sem, to, when)
        count[p] += 1

    def wait_block(p, block, piece=None):
        piece = whole if piece is None else piece
        arrived(held.at[p, block, piece], w_recv.at[p, block, 1 if piece is second else 0])

    locals_ = []

    def issue_own(p):
        if p >= phases:
            return
        send_own(p, along(up), has_up)
        send_own(p, along(down), has_down)
        send_own(p, y_mate)
        send_own(p, c_mate)
        copy = pltpu.make_async_copy(own(p), held.at[p, s], local_sem.at[p])
        copy.start()
        locals_.append(copy)

    def take_mate(p):
        block = block_of(z, 1 - y, core)
        wait_block(p, block)
        forward(p, block, along(inner), second, at_end)
        forward(p, block, c_mate)

    def take_near(p):
        block = block_of(near, y, core)
        wait_block(p, block)
        forward(p, block, along(inner), None, inside)
        forward(p, block, y_mate, first)
        forward(p, block, y_mate, second, at_end)
        forward(p, block, c_mate)

    def take_across(p):
        block = block_of(across, y, core)
        wait_block(p, block)
        forward(p, block, along(outer), None, inside)
        forward(p, block, y_mate)
        forward(p, block, c_mate)

    def take_far(p):
        block = block_of(far, y, core)
        wait_block(p, block)
        forward(p, block, along(outer), None, inside)
        forward(p, block, y_mate, first)
        forward(p, block, c_mate)

    def take_mate_near(p):
        block = block_of(near, 1 - y, core)
        wait_block(p, block, second)
        forward(p, block, along(inner), second, inside)
        wait_block(p, block, first)
        forward(p, block, c_mate)

    def take_mate_across(p):
        block = block_of(across, 1 - y, core)
        wait_block(p, block)
        forward(p, block, c_mate)

    def take_mate_far(p):
        block = block_of(far, 1 - y, core)
        wait_block(p, block, second)
        forward(p, block, along(outer), second, inside)
        wait_block(p, block, first)
        forward(p, block, c_mate)

    def finish(p):
        locals_[p].wait()
        for zz in range(n_z):
            for yy in range(2):
                wait_block(p, block_of(zz, yy, 1 - core))

    send(x_ref.at[pl.ds(rows - halo, halo)], edge, a_send.at[0], a_recv.at[0], after)
    issue_own(0)
    issue_own(1)

    @pl.loop(0, rows // REACH)
    def _(i):
        state[pl.ds(halo + i * REACH, REACH)] = x_ref[pl.ds(i * REACH, REACH)]

    arrived(edge, a_recv.at[0])
    keep = (s > 0).astype(jnp.float32)

    @pl.loop(0, halo // REACH)
    def _(i):
        part = edge[pl.ds(i * REACH, REACH)].astype(jnp.float32) * keep
        state[pl.ds(i * REACH, REACH)] = part.astype(jnp.bfloat16)

    def first_row(layer):
        return REACH * layer

    def from_row(start):
        return pl.ds(start, total - start)

    parts = mix.shape[2]
    slim = mix.shape[4]
    ahead = blocks // (2 * parts)

    def exchange(src, dst, sem):
        send(src, dst, a_send.at[sem], a_recv.at[sem], x_mate)

    def base_sem(layer):
        return 1 + (1 + 2 * parts) * layer

    def squares(layer):
        @pl.loop(first_row(layer) // REACH, total // REACH)
        def _(i):
            at = pl.ds(i * REACH, REACH)
            wide = state[at].astype(jnp.float32)
            value = jnp.sum(wide * wide, axis=1, keepdims=True)
            sq_send[layer, at] = jnp.broadcast_to(value, (REACH, 128))
            gain = gain_ref[pl.ds(layer, 1), pl.ds(pl.multiple_of(t * feats, 128), feats)]
            xg[at] = (wide * gain).astype(jnp.bfloat16)

        at = from_row(first_row(layer))
        exchange(sq_send.at[layer, at], sq_recv.at[layer, at], base_sem(layer))

    def project(layer, which, c):
        block = which * (blocks // 2) + c * ahead
        weight = held[2 * layer, pl.ds(block, ahead)].reshape(slim, feats)
        return lax.dot_general(
            xg[first_row(layer):], weight, (((1,), (1,)), ((), ())),
            preferred_element_type=jnp.float32,
        )

    def project_other(layer, c):
        at = from_row(first_row(layer))
        p_send[layer, c, at] = project(layer, 1 - t, c).astype(jnp.bfloat16)
        exchange(p_send.at[layer, c, at], p_recv.at[layer, c, at], base_sem(layer) + 1 + c)

    def project_own(layer, c):
        p_own[c, from_row(first_row(layer))] = project(layer, t, c)

    def pool(layer, c):
        sem = base_sem(layer)
        start = first_row(layer)
        at = from_row(start)
        if c == 0:
            arrived(sq_recv.at[layer, at], a_recv.at[sem])
        arrived(p_recv.at[layer, c, at], a_recv.at[sem + 1 + c])
        lanes = 128
        row = lax.broadcasted_iota(jnp.int32, (total - start, lanes), 0)
        position = s * rows - halo + start + row
        mean = (sq_send[layer, at] + sq_recv[layer, at]) / (2 * feats)
        inv = lax.rsqrt(mean + EPS)
        for j in range(slim // lanes):
            cols = pl.ds(j * lanes, lanes)
            joined = p_own[c, at, cols].astype(jnp.bfloat16).astype(jnp.float32)
            joined = joined + p_recv[layer, c, at, cols].astype(jnp.float32)
            base = (joined * inv).astype(jnp.bfloat16).astype(jnp.float32)
            lane = t * half + c * slim + j * lanes
            channel = lane + lax.broadcasted_iota(jnp.int32, (1, lanes), 1)
            group = channel // (pools // GROUPS)
            running = base
            width = 1
            picked = None
            for g in range(GROUPS):
                running = running + pltpu.roll(running, width, 0)
                width *= 2
                picked = running if picked is None else jnp.where(group >= g, running, picked)
            span = jnp.left_shift(jnp.int32(2), group)
            divisor = jnp.maximum(jnp.minimum(position + 1, span), 1).astype(jnp.float32)
            scale = scale_ref[pl.ds(layer, 1), pl.ds(pl.multiple_of(lane, 128), lanes)]
            mix[layer, t, c, at, cols] = ((picked / divisor - base) * scale).astype(jnp.bfloat16)
        at = from_row(first_row(layer + 1))
        exchange(mix.at[layer, t, c, at], mix.at[layer, t, c, at], sem + 1 + parts + c)

    def take_mix(layer):
        at = from_row(first_row(layer + 1))
        for c in range(parts):
            arrived(mix.at[layer, 1 - t, c, at], a_recv.at[base_sem(layer) + 1 + parts + c])

    def expand(layer, start, stop):
        p = 2 * layer + 1
        width = 256
        last = layer == layers - 1
        at = from_row(first_row(layer + 1))

        @pl.loop(start, stop)
        def _(n):
            cols = pl.ds(pl.multiple_of(n * width, width), width)
            mixed = jnp.concatenate(
                [mix[layer, h, c, at] for h in range(2) for c in range(parts)], axis=1
            )
            weight = held[p, :, :, cols].reshape(pools, width)
            branch = jnp.dot(mixed, weight, preferred_element_type=jnp.float32)
            new = (state[at, cols].astype(jnp.float32) + branch).astype(jnp.bfloat16)
            if last:
                o_ref[:, cols] = new
            else:
                state[at, cols] = new

    part = functools.partial

    def pieces(p):
        layer = p // 2
        if p % 2 == 0:
            todo = [part(project_other, layer, c) for c in range(parts)]
            todo += [part(project_own, layer, c) for c in range(parts)]
            return todo + [part(pool, layer, c) for c in range(parts)]
        columns = feats // 256
        step = columns // 4
        todo = [part(take_mix, layer)]
        todo += [part(expand, layer, k, k + step) for k in range(0, columns, step)]
        if layer + 1 < layers:
            todo.append(part(squares, layer + 1))
        return todo

    order_first = [take_mate, take_near, take_across, take_far]
    order_then = [take_mate_near, take_mate_across, take_mate_far, finish]
    waiting = []

    def work():
        if waiting:
            piece = waiting.pop(0)
            if piece is not None:
                piece()

    squares(0)
    for take in order_first:
        take(0)
    for p in range(phases):
        issue_own(p + 2)
        for take in order_first[:2]:
            if p + 1 < phases:
                take(p + 1)
                work()
        for take in order_then[:2]:
            take(p)
            work()
        for take in order_first[2:]:
            if p + 1 < phases:
                take(p + 1)
                work()
        for take in order_then[2:]:
            take(p)
            work()
        waiting.extend(pieces(p))
        work()
        if p % 2 == 0:
            work()
            work()
            work()
    while waiting:
        work()
    for copy, when in sent:
        if when is None:
            copy.wait_send()
        else:
            pl.when(when)(copy.wait_send)


def fused_body(inputs, norm_gain, in_weight, pool_scale, out_weight):
    rows, feats = inputs.shape
    layers = norm_gain.shape[0]
    half = pool_scale.shape[1] // 2
    blocks = lax.axis_size("sp")
    n_z = blocks // 4
    depth = out_weight.shape[1]
    halo = REACH * layers
    total = rows + halo
    bf, f32 = jnp.bfloat16, jnp.float32
    sends = 21
    parts = 2
    slim = half // parts
    vmem = pl.BlockSpec(memory_space=pltpu.VMEM)
    return pl.pallas_call(
        functools.partial(kernel, n_z, layers, halo),
        out_shape=jax.ShapeDtypeStruct((rows, feats), bf),
        in_specs=[vmem] * 5,
        out_specs=vmem,
        scratch_shapes=[
            pltpu.VMEM((2 * layers, blocks, depth, feats), bf),
            pltpu.VMEM((total, feats), bf),
            pltpu.VMEM((total, feats), bf),
            pltpu.VMEM((halo, feats), bf),
            pltpu.VMEM((parts, total, slim), f32),
            pltpu.VMEM((layers, parts, total, slim), bf),
            pltpu.VMEM((layers, parts, total, slim), bf),
            pltpu.VMEM((layers, 2, parts, total, slim), bf),
            pltpu.VMEM((layers, total, 128), f32),
            pltpu.VMEM((layers, total, 128), f32),
            pltpu.SemaphoreType.DMA((2 * layers, sends)),
            pltpu.SemaphoreType.DMA((2 * layers, blocks, 2)),
            pltpu.SemaphoreType.DMA((2 * layers,)),
            pltpu.SemaphoreType.DMA((1 + (1 + 2 * parts) * layers,)),
            pltpu.SemaphoreType.DMA((1 + (1 + 2 * parts) * layers,)),
        ],
        compiler_params=pltpu.CompilerParams(
            collective_id=0, has_side_effects=True, vmem_limit_bytes=60 * 1024 * 1024
        ),
    )(inputs, norm_gain, jnp.swapaxes(in_weight, 1, 2), pool_scale, out_weight)


def solution(mesh):
    n_sp, n_tp = mesh.shape["sp"], mesh.shape["tp"]
    fused = n_tp == 2 and n_sp == 16
    placed = (P("sp", "tp"), P(), P(None, "tp", "sp"), P(), P(None, "sp", "tp"))
    return jax.shard_map(
        fused_body if fused else plain_body,
        mesh=mesh, in_specs=placed, out_specs=P("sp", "tp"), check_vma=False,
    )
```

profile of v0, /device:TPU:0, one launch (start us, length us, event | category | flops | bytes accessed | tf_op | source)
XLA Modules:
  0.0 149.3 jit_solution(4735187431852211860)
XLA Ops:
  0.0 147.0 %shard_map.55 = bf16[256,2048]{1,0:T(8,128)(2,1)} custom-call(bf16[256,2048]{1,0:T(8,128)(2,1)} %x_ref.1, f32[3,4096]{1,0:T(4,128)} %gain_ref.1, bf16[3,64,2048]{2,1,0:T(8,128)(2,1)} %bitcast.1, f32[3,1024]{1,0:T(4,128)} %scale_ref.1, bf16[3,64,2048]{2,1,0:T(8,128)(2,1)} %wo_ref.1), custom_call_target="tpu_custom_call" | custom-call | tf_op jit(solution)/shard_map/pallas_call | solution.py:414
  147.0 2.3 %copy.7 = bf16[256,2048]{1,0:T(8,128)(2,1)} copy(bf16[256,2048]{1,0:T(8,128)(2,1)} %shard_map.55) | data formatting | bytes 2097152
where the time goes:
time: 151 us; the launch traced here: 149 us
  Pallas kernels  147 us (97%)
  local copies, waits for them, and re-layouts  2.3 us (2%)
    pallas_call x1, Pallas kernels, fused_body(): pl.pallas_call(functools.partial(kernel, n_z, layers, halo), out_shape=ja...  147 us

commit v1 on v0

v1 whole, which is shorter than its diff:
```python
import functools

import jax
import jax.numpy as jnp
from jax import lax
from jax.experimental import pallas as pl
from jax.experimental.pallas import tpu as pltpu
from jax.sharding import PartitionSpec as P

EPS = 1e-06
REACH = 16
GROUPS = 4
MESH_ID = pl.DeviceIdType.MESH


def shift_sp(value):
    count = lax.axis_size("sp")
    return lax.ppermute(value, "sp", [(i, i + 1) for i in range(count - 1)])


def window_means(extended, row_count, first_channel, first_pos, pool_total):
    width = extended.shape[1]
    channel = first_channel + lax.broadcasted_iota(jnp.int32, (1, width), 1)
    window_len = jnp.left_shift(jnp.int32(2), channel // (pool_total // GROUPS))
    running = jnp.zeros((row_count, width), jnp.float32)
    for offset in range(REACH):
        shifted = extended[REACH - offset : REACH - offset + row_count]
        running = running + jnp.where(offset < window_len, shifted, 0.0)
    position = first_pos + lax.broadcasted_iota(jnp.int32, (row_count, 1), 0)
    divisor = jnp.minimum(position + 1, window_len).astype(jnp.float32)
    return running / divisor - extended[REACH:]


def plain_body(inputs, norm_gain, in_weight, pool_scale, out_weight):
    rows, feats = inputs.shape
    layers, features = norm_gain.shape
    pools = pool_scale.shape[1]
    part = pools // lax.axis_size("tp")
    t = lax.axis_index("tp")
    s = lax.axis_index("sp")
    current = inputs
    for layer in range(layers):
        in_all = lax.all_gather(in_weight[layer], "sp", axis=1, tiled=True)
        out_all = lax.all_gather(out_weight[layer], "sp", axis=0, tiled=True)
        wide = current.astype(jnp.float32)
        squares = lax.psum(jnp.sum(wide * wide, axis=1), "tp")
        inv_rms = lax.rsqrt(squares / features + EPS)[:, None]
        gain = lax.dynamic_slice_in_dim(norm_gain[layer], t * feats, feats)
        normed = (wide * inv_rms * gain).astype(jnp.bfloat16)
        partial = jnp.dot(normed, in_all, preferred_element_type=jnp.float32)
        pool_in = lax.psum_scatter(
            partial.astype(jnp.bfloat16), "tp", scatter_dimension=1, tiled=True
        )
        edge = shift_sp(pool_in[rows - REACH :])
        extended = jnp.concatenate([edge, pool_in], 0).astype(jnp.float32)
        means = window_means(extended, rows, t * part, s * rows, pools)
        scale = lax.dynamic_slice_in_dim(pool_scale[layer], t * part, part)
        mixed = (means * scale).astype(jnp.bfloat16)
        pooled = lax.all_gather(mixed, "tp", axis=1, tiled=True)
        branch = jnp.dot(pooled, out_all, preferred_element_type=jnp.float32)
        current = (current.astype(jnp.float32) + branch).astype(jnp.bfloat16)
    return current


PIECES = 4
STATE_CHUNKS = 4


def phase_table(layers, feats):
    table = []
    for layer in range(layers):
        table.append((2 * layer, 0, feats))
        count = PIECES if layer == layers - 1 else 1
        width = feats // count
        table += [(2 * layer + 1, k * width, width) for k in range(count)]
    return table


def kernel(
    n_z, layers, halo,
    x_ref, gain_ref, wi_ref, scale_ref, wo_ref, o_ref,
    held, state, xg, edge, p_send, p_recv, mix, stage, part_sq, inv_col, sq_send, sq_recv,
    w_send, w_recv, local_sem, e_send, e_recv, s_send, s_recv, a_send, a_recv, f_send, f_recv,
):
    rows, feats = x_ref.shape
    total = rows + halo
    blocks, depth = held.shape[1], held.shape[2]
    pools = scale_ref.shape[1]
    chunk = pools // n_z
    last = layers - 1
    table = phase_table(layers, feats)
    phases = len(table)
    lanes = 128
    sq_tiles = part_sq.shape[1] // lanes
    s = lax.axis_index("sp")
    t = lax.axis_index("tp")
    core = s % 2
    y = (s // 2) % 2
    z = s // 4
    side = z // 2

    def block_of(zz, yy, cc):
        return zz * 4 + yy * 2 + cc

    z_in, z_end = 1 + side, 3 * side
    z_over, z_far = 2 - side, 3 - 3 * side
    is_end = z == z_end
    s_end, s_in = block_of(z_end, y, core), block_of(z_in, y, core)

    y_mate = (block_of(z, 1 - y, core), t)
    c_mate = (block_of(z, y, 1 - core), t)
    x_mate = (s, 1 - t)
    opposite = (block_of(z_over, y, core), t)
    inner = (s_in, t)
    outer = (s_end, t)
    after = (s + 1) % blocks
    after_z = after // 4
    after_holder = (block_of(1 + after_z // 2, (after // 2) % 2, after % 2), t)
    after_slot = jnp.where((after_z == 0) | (after_z == n_z - 1), 1, 0)
    before = [((s_in + blocks - 1) % blocks, t), ((s_end + blocks - 1) % blocks, t)]

    barrier = pltpu.get_barrier_semaphore()

    def greet(peers):
        for peer in peers:
            pl.semaphore_signal(barrier, inc=1, device_id=peer, device_id_type=MESH_ID)

    sent = []

    def send(src, dst, send_sem, recv_sem, to):
        copy = pltpu.make_async_remote_copy(
            src_ref=src, dst_ref=dst, send_sem=send_sem, recv_sem=recv_sem,
            device_id=to, device_id_type=MESH_ID,
        )
        copy.start()
        sent.append(copy)

    def arrived(ref, sem):
        pltpu.make_async_remote_copy(
            src_ref=ref, dst_ref=ref, send_sem=sem, recv_sem=sem,
            device_id=c_mate, device_id_type=MESH_ID,
        ).wait_recv()

    whole, first, second = pl.ds(0, depth), pl.ds(0, depth // 2), pl.ds(depth // 2, depth // 2)
    count = [0] * phases

    def own(ph):
        buf, start, width = table[ph]
        return (wi_ref if buf % 2 == 0 else wo_ref).at[buf // 2, :, pl.ds(start, width)]

    def slot(ph, block, piece=whole):
        buf, start, width = table[ph]
        return held.at[buf, block, piece, pl.ds(start, width)]

    def recv_sem(ph, block, piece=whole):
        return w_recv.at[ph, block, 1 if piece is second else 0]

    def next_send(ph):
        count[ph] += 1
        return w_send.at[ph, count[ph] - 1]

    def send_own(ph, to):
        send(own(ph), slot(ph, s), next_send(ph), recv_sem(ph, s), to)

    def forward(ph, block, to, piece=whole):
        ref = slot(ph, block, piece)
        send(ref, ref, next_send(ph), recv_sem(ph, block, piece), to)

    def wait_block(ph, block, piece=whole):
        arrived(slot(ph, block, piece), recv_sem(ph, block, piece))

    state_rows = rows // STATE_CHUNKS
    final_cols = feats // PIECES

    def send_edge():
        send(
            x_ref.at[pl.ds(rows - halo, halo)], edge.at[after_slot],
            e_send.at[0], e_recv.at[after_slot], after_holder,
        )

    def end_program():
        greet([inner, y_mate])
        pl.semaphore_wait(barrier, 3)
        mate = block_of(z, 1 - y, core)

        def ship(k):
            at = pl.ds(k * state_rows, state_rows)
            send(
                x_ref.at[at], state.at[1, pl.ds(halo + k * state_rows, state_rows)],
                s_send.at[k], s_recv.at[k], inner,
            )

        send_own(0, y_mate)
        send_own(0, inner)
        send_edge()
        send_own(1, y_mate)
        wait_block(0, mate)
        forward(0, mate, inner)
        for k in range(STATE_CHUNKS):
            ship(k)
        for ph in range(1, phases):
            send_own(ph, inner)
            if ph + 1 < phases:
                send_own(ph + 1, y_mate)
            wait_block(ph, mate)
            forward(ph, mate, inner)
        for k in range(PIECES):
            at = pl.ds(k * final_cols, final_cols)
            arrived(o_ref.at[:, at], f_recv.at[k])
        for copy in sent:
            copy.wait_send()
        sent.clear()

    def inner_program():
        greet([opposite, y_mate, c_mate, x_mate, outer] + before)
        pl.semaphore_wait(barrier, 6)
        locals_ = {}
        chunk_z = [z_in, z_end, z_over, z_far]

        def issue(ph):
            if ph >= phases:
                return
            send_own(ph, opposite)
            send_own(ph, y_mate)
            send_own(ph, c_mate)
            copy = pltpu.make_async_copy(own(ph), slot(ph, s), local_sem.at[ph])
            copy.start()
            locals_[ph] = copy

        def take_end(ph):
            block = block_of(z_end, y, core)
            wait_block(ph, block)
            forward(ph, block, opposite)
            forward(ph, block, c_mate)

        def take_over(ph):
            block = block_of(z_over, y, core)
            wait_block(ph, block)
            forward(ph, block, y_mate, first)
            forward(ph, block, c_mate)

        def take_mate(ph):
            block = block_of(z_in, 1 - y, core)
            wait_block(ph, block)
            forward(ph, block, opposite, second)
            forward(ph, block, c_mate)

        def take_far(ph):
            block = block_of(z_far, y, core)
            wait_block(ph, block)
            forward(ph, block, y_mate)
            forward(ph, block, c_mate)

        def take_mate_end(ph):
            block = block_of(z_end, 1 - y, core)
            wait_block(ph, block)
            forward(ph, block, c_mate)

        def take_mate_over(ph):
            block = block_of(z_over, 1 - y, core)
            wait_block(ph, block, first)
            wait_block(ph, block, second)
            forward(ph, block, c_mate)

        def take_mate_far(ph):
            block = block_of(z_far, 1 - y, core)
            wait_block(ph, block)
            forward(ph, block, c_mate)

        def plane(ph, k):
            if k == 0:
                locals_[ph].wait()
            for yy in range(2):
                wait_block(ph, block_of(chunk_z[k], yy, 1 - core))

        def first_row(layer):
            return REACH * layer

        def from_row(start):
            return pl.ds(start, total - start)

        def gain_of(layer, start, width):
            at = pl.multiple_of(t * feats + start, lanes)
            return gain_ref[pl.ds(layer, 1), pl.ds(at, width)]

        def pack_squares(g, layer):
            for k in range(sq_tiles):
                block = part_sq[g, pl.ds(k * lanes, lanes)].T
                value = jnp.sum(block, axis=0, keepdims=True)
                sq_send[layer, g, k] = jnp.broadcast_to(value, (8, lanes))
            exchange(sq_send.at[layer, g], sq_recv.at[layer, g], layer, g, n_z)

        def exchange(src, dst, layer, g, k):
            send(src, dst, a_send.at[layer, g, k], a_recv.at[layer, g, k], x_mate)

        def take_edge(g):
            arrived(edge.at[g], e_recv.at[g])
            keep = ((s_in if g == 0 else s_end) > 0).astype(jnp.float32)

            @pl.loop(0, halo // REACH)
            def _(i):
                at = pl.ds(i * REACH, REACH)
                state[g, at] = (edge[g, at].astype(jnp.float32) * keep).astype(jnp.bfloat16)

        def own_state():
            @pl.loop(0, rows // REACH)
            def _(i):
                state[0, pl.ds(halo + i * REACH, REACH)] = x_ref[pl.ds(i * REACH, REACH)]

        def take_state(k):
            arrived(state.at[1, pl.ds(halo + k * state_rows, state_rows)], s_recv.at[k])

        def squares(g, start, stop):
            @pl.loop(start // REACH, stop // REACH)
            def _(i):
                at = pl.ds(i * REACH, REACH)
                sums = jnp.zeros((REACH, lanes), jnp.float32)
                for j in range(feats // lanes):
                    cols = pl.ds(j * lanes, lanes)
                    wide = state[g, at, cols].astype(jnp.float32)
                    sums = sums + wide * wide
                    xg[g, at, cols] = (wide * gain_of(0, j * lanes, lanes)).astype(jnp.bfloat16)
                part_sq[g, at] = sums

        def project(layer, g, k):
            at = from_row(first_row(layer))
            weight = held[2 * layer, pl.ds(chunk_z[k] * 4, 4)].reshape(chunk, feats)
            value = lax.dot_general(
                xg[g, at], weight, (((1,), (1,)), ((), ())),
                preferred_element_type=jnp.float32,
            )
            p_send[layer, g, k, at] = value.astype(jnp.bfloat16)
            exchange(p_send.at[layer, g, k, at], p_recv.at[layer, g, k, at], layer, g, k)

        def inverse(layer, g):
            arrived(sq_recv.at[layer, g], a_recv.at[layer, g, n_z])
            for k in range(sq_tiles):
                mean = (sq_send[layer, g, k] + sq_recv[layer, g, k]) / (2 * feats)
                inv = lax.rsqrt(mean + EPS)
                inv_col[g, pl.ds(k * lanes, lanes)] = jnp.broadcast_to(inv[0:1], (lanes, lanes)).T

        def pool(layer, g, k):
            start = first_row(layer)
            at = from_row(start)
            arrived(p_recv.at[layer, g, k, at], a_recv.at[layer, g, k])
            group = chunk_z[k]
            row = lax.broadcasted_iota(jnp.int32, (total - start, lanes), 0)
            position = (s_in if g == 0 else s_end) * rows - halo + start + row
            span = jnp.left_shift(jnp.int32(2), group)
            divisor = jnp.maximum(jnp.minimum(position + 1, span), 1).astype(jnp.float32)
            share = 1.0 / divisor
            inv = inv_col[g, at]
            for j in range(chunk // lanes):
                cols = pl.ds(j * lanes, lanes)
                joined = p_send[layer, g, k, at, cols].astype(jnp.float32)
                joined = joined + p_recv[layer, g, k, at, cols].astype(jnp.float32)
                base = (joined * inv).astype(jnp.bfloat16).astype(jnp.float32)
                running = base
                width = 1
                picked = None
                for step in range(GROUPS):
                    running = running + pltpu.roll(running, width, 0)
                    width *= 2
                    picked = running if picked is None else jnp.where(group >= step, running, picked)
                lane = pl.multiple_of(group * chunk + j * lanes, lanes)
                scale = scale_ref[pl.ds(layer, 1), pl.ds(lane, lanes)]
                mix[g, group, at, cols] = ((picked * share - base) * scale).astype(jnp.bfloat16)

        def expand(layer, g, start, stop):
            width = 256
            at = from_row(first_row(layer + 1))
            buf = 2 * layer + 1

            @pl.loop(start // width, stop // width)
            def _(n):
                col = pl.multiple_of(n * width, width)
                cols = pl.ds(col, width)
                mixed = jnp.concatenate([mix[g, c, at] for c in range(n_z)], axis=1)
                weight = held[buf, :, :, cols].reshape(pools, width)
                branch = jnp.dot(mixed, weight, preferred_element_type=jnp.float32)
                new = (state[g, at, cols].astype(jnp.float32) + branch).astype(jnp.bfloat16)
                if layer == last:
                    if g == 0:
                        o_ref[:, cols] = new
                    else:
                        stage[:, cols] = new
                else:
                    state[g, at, cols] = new
                    wide = new.astype(jnp.float32)
                    xg[g, at, cols] = (wide * gain_of(layer + 1, col, width)).astype(jnp.bfloat16)
                    square = wide * wide
                    sums = square[:, :lanes]
                    for j in range(1, width // lanes):
                        sums = sums + square[:, j * lanes:(j + 1) * lanes]
                    part_sq[g, at] = part_sq[g, at] + sums

        def clear(g):
            part_sq[g] = jnp.zeros(part_sq.shape[1:], jnp.float32)

        def return_final(k):
            cols = pl.ds(k * final_cols, final_cols)
            send(stage.at[:, cols], o_ref.at[:, cols], f_send.at[k], f_recv.at[k], outer)

        def early(ph):
            take_end(ph)
            take_over(ph)
            take_mate(ph)

        def middle(ph):
            take_far(ph)
            take_mate_end(ph)

        def late(ph):
            take_mate_over(ph)
            take_mate_far(ph)

        def planes(ph):
            for k in range(n_z):
                plane(ph, k)

        a_of = [i for i, row in enumerate(table) if row[0] % 2 == 0]
        b_of = [[i for i, row in enumerate(table) if row[0] == 2 * l + 1] for l in range(layers)]

        send_edge()
        issue(0)
        issue(1)
        clear(0)
        clear(1)
        own_state()
        take_edge(0)
        squares(0, 0, total)
        pack_squares(0, 0)
        early(0)
        plane(0, 0)
        project(0, 0, 0)
        middle(0)
        plane(0, 1)
        project(0, 0, 1)
        issue(2)
        early(1)
        late(0)
        plane(0, 2)
        project(0, 0, 2)
        plane(0, 3)
        project(0, 0, 3)
        inverse(0, 0)
        pool(0, 0, 0)
        take_edge(1)
        squares(1, 0, halo)
        middle(1)
        for k in range(2):
            take_state(k)
            squares(1, halo + k * state_rows, halo + (k + 1) * state_rows)
        pool(0, 0, 1)
        issue(3)
        late(1)
        pool(0, 0, 2)
        for k in range(2, STATE_CHUNKS):
            take_state(k)
            squares(1, halo + k * state_rows, halo + (k + 1) * state_rows)
        pack_squares(1, 0)
        project(0, 1, 0)
        project(0, 1, 1)
        early(2)
        project(0, 1, 2)
        project(0, 1, 3)
        pool(0, 0, 3)
        clear(0)
        planes(1)
        expand(0, 0, 0, feats)
        pack_squares(0, 1)
        middle(2)
        issue(4)
        plane(2, 0)
        project(1, 0, 0)
        plane(2, 1)
        project(1, 0, 1)
        early(3)
        late(2)
        plane(2, 2)
        project(1, 0, 2)
        inverse(0, 1)
        pool(0, 1, 0)
        plane(2, 3)
        project(1, 0, 3)
        for k in range(1, n_z):
            pool(0, 1, k)
        clear(1)
        middle(3)
        expand(0, 1, 0, feats)
        pack_squares(1, 1)
        issue(5)
        for k in range(n_z):
            project(1, 1, k)
        late(3)
        early(4)
        inverse(1, 0)
        for k in range(n_z):
            pool(1, 0, k)
        planes(3)
        clear(0)
        middle(4)
        issue(6)
        expand(1, 0, 0, feats)
        pack_squares(0, 2)
        plane(4, 0)
        project(2, 0, 0)
        plane(4, 1)
        project(2, 0, 1)
        early(5)
        inverse(1, 1)
        for k in range(n_z):
            pool(1, 1, k)
        clear(1)
        expand(1, 1, 0, feats)
        pack_squares(1, 2)
        project(2, 1, 0)
        project(2, 1, 1)
        late(4)
        plane(4, 2)
        project(2, 0, 2)
        project(2, 1, 2)
        plane(4, 3)
        project(2, 1, 3)
        project(2, 0, 3)
        middle(5)
        issue(7)
        early(6)
        inverse(2, 1)
        pool(2, 1, 0)
        late(5)
        pool(2, 1, 1)
        middle(6)
        issue(8)
        pool(2, 1, 2)
        early(7)
        late(6)
        pool(2, 1, 3)
        for piece in range(PIECES):
            ph = b_of[last][piece]
            planes(ph)
            expand(last, 1, piece * final_cols, (piece + 1) * final_cols)
            return_final(piece)
            if piece == 0:
                inverse(2, 0)
                pool(2, 0, 0)
                pool(2, 0, 1)
                middle(7)
                early(8)
                late(7)
            if piece == 1:
                pool(2, 0, 2)
                pool(2, 0, 3)
                middle(8)
                late(8)
        expand(last, 0, 0, feats)
        for copy in sent:
            copy.wait_send()
        sent.clear()

    pl.when(is_end)(end_program)
    for ph in range(phases):
        count[ph] = 0
    pl.when(jnp.logical_not(is_end))(inner_program)


def fused_body(inputs, norm_gain, in_weight, pool_scale, out_weight):
    rows, feats = inputs.shape
    layers = norm_gain.shape[0]
    pools = pool_scale.shape[1]
    blocks = lax.axis_size("sp")
    n_z = blocks // 4
    depth = out_weight.shape[1]
    halo = REACH * layers
    total = rows + halo
    sq_tiles = -(-total // 128)
    chunk = pools // n_z
    phases = len(phase_table(layers, feats))
    bf, f32 = jnp.bfloat16, jnp.float32
    vmem = pl.BlockSpec(memory_space=pltpu.VMEM)
    dma = pltpu.SemaphoreType.DMA
    return pl.pallas_call(
        functools.partial(kernel, n_z, layers, halo),
        out_shape=jax.ShapeDtypeStruct((rows, feats), bf),
        in_specs=[vmem] * 5,
        out_specs=vmem,
        scratch_shapes=[
            pltpu.VMEM((2 * layers, blocks, depth, feats), bf),
            pltpu.VMEM((2, total, feats), bf),
            pltpu.VMEM((2, total, feats), bf),
            pltpu.VMEM((2, halo, feats), bf),
            pltpu.VMEM((layers, 2, n_z, total, chunk), bf),
            pltpu.VMEM((layers, 2, n_z, total, chunk), bf),
            pltpu.VMEM((2, n_z, total, chunk), bf),
            pltpu.VMEM((rows, feats), bf),
            pltpu.VMEM((2, sq_tiles * 128, 128), f32),
            pltpu.VMEM((2, sq_tiles * 128, 128), f32),
            pltpu.VMEM((layers, 2, sq_tiles, 8, 128), f32),
            pltpu.VMEM((layers, 2, sq_tiles, 8, 128), f32),
            dma((phases, 14)),
            dma((phases, blocks, 2)),
            dma((phases,)),
            dma((1,)),
            dma((2,)),
            dma((STATE_CHUNKS,)),
            dma((STATE_CHUNKS,)),
            dma((layers, 2, n_z + 1)),
            dma((layers, 2, n_z + 1)),
            dma((PIECES,)),
            dma((PIECES,)),
        ],
        compiler_params=pltpu.CompilerParams(
            collective_id=0, has_side_effects=True, vmem_limit_bytes=60 * 1024 * 1024
        ),
    )(inputs, norm_gain, jnp.swapaxes(in_weight, 1, 2), pool_scale, out_weight)


def solution(mesh):
    n_sp, n_tp = mesh.shape["sp"], mesh.shape["tp"]
    fused = n_tp == 2 and n_sp == 16
    placed = (P("sp", "tp"), P(), P(None, "tp", "sp"), P(), P(None, "sp", "tp"))
    return jax.shard_map(
        fused_body if fused else plain_body,
        mesh=mesh, in_specs=placed, out_specs=P("sp", "tp"), check_vma=False,
    )
```

time: 151 us -> 162 us (1.073); the launches traced: 149 us -> 162 us
  Pallas kernels: 147 us -> 160 us
    pallas_call x1, Pallas kernels: 147 us -> 160 us  [fused_body(): pl.pallas_call(functools.partial(kernel, n_z, layers, halo), out_shape=ja...]
where the time goes in v1:
time: 162 us
  Pallas kernels  160 us (99%)
  local copies, waits for them, and re-layouts  2.3 us (1%)
    pallas_call x1, Pallas kernels, fused_body(): pl.pallas_call(functools.partial(kernel, n_z, layers, halo), out_shape=ja...  160 us

profile of v1, /device:TPU:0, one launch (start us, length us, event | category | flops | bytes accessed | tf_op | source)
XLA Modules:
  0.0 162.0 jit_solution(7189540263420353018)
XLA Ops:
  0.0 159.7 %shard_map.55 = bf16[256,2048]{1,0:T(8,128)(2,1)} custom-call(bf16[256,2048]{1,0:T(8,128)(2,1)} %x_ref.1, f32[3,4096]{1,0:T(4,128)} %gain_ref.1, bf16[3,64,2048]{2,1,0:T(8,128)(2,1)} %bitcast.1, f32[3,1024]{1,0:T(4,128)} %scale_ref.1, bf16[3,64,2048]{2,1,0:T(8,128)(2,1)} %wo_ref.1), custom_call_target="tpu_custom_call" | custom-call | tf_op jit(solution)/shard_map/pallas_call | solution.py:582
  159.7 2.3 %copy.7 = bf16[256,2048]{1,0:T(8,128)(2,1)} copy(bf16[256,2048]{1,0:T(8,128)(2,1)} %shard_map.55) | data formatting | bytes 2097152

commit v2 on v1

--- a/solution.py
+++ b/solution.py
@@ -62,25 +62,69 @@
     return current
 
 
-PIECES = 4
-STATE_CHUNKS = 4
-
-
-def phase_table(layers, feats):
+PIECES = (2, 2, 2, 2, 2, 4)
+EDGE_BY_MATE = (True, True, False, False, False, False)
+OVER_BY_MATE = (0.5, 0, 0.5, 1, 0, 0.5)
+INNER_ORDER = [
+    ("init",), ("issue", 0), ("issue", 1), ("issue", 2), ("sq", 0), ("M", 0), ("O", 0), ("E", 0), ("inv", 0, 0),
+    ("O", 1), ("M", 1), ("plane", 0, 0), ("P", 0, 0, 0), ("st", 0), ("M", 2), ("O", 2), ("OM", 0), ("E", 1),
+    ("F", 0), ("EM", 0), ("issue", 3), ("Q", 0, 0, 0), ("OM", 1), ("plane", 0, 2), ("P", 0, 0, 2), ("st", 1),
+    ("EM", 1), ("OM", 2), ("plane", 0, 1), ("P", 0, 0, 1), ("FM", 0), ("F", 1), ("issue", 4), ("Q", 0, 0, 2),
+    ("st", 2), ("M", 3), ("O", 3), ("plane", 1, 0), ("Q", 0, 0, 1), ("E", 2), ("FM", 1), ("O", 4), ("plane", 0, 3),
+    ("P", 0, 0, 3), ("E", 3), ("OM", 3), ("M", 4), ("plane", 1, 2), ("EM", 2), ("F", 2), ("issue", 5),
+    ("Q", 0, 0, 3), ("st", 3), ("sq", 1), ("F", 3), ("issue", 6), ("P", 0, 1, 2), ("P", 0, 1, 1), ("EM", 3),
+    ("OM", 4), ("P", 0, 1, 3), ("E", 4), ("P", 0, 1, 0), ("plane", 1, 1), ("inv", 0, 1), ("O", 5), ("FM", 2),
+    ("EM", 4), ("Q", 0, 1, 2), ("O", 6), ("M", 5), ("E", 5), ("plane", 2, 0), ("Q", 0, 1, 1), ("FM", 3), ("F", 4),
+    ("issue", 7), ("EM", 5), ("plane", 1, 3), ("X", 0, 0, 0, 2), ("M", 6), ("plane", 2, 1), ("X", 0, 0, 2, 3),
+    ("Q", 0, 1, 3), ("X", 0, 0, 3, 4), ("E", 6), ("F", 5), ("issue", 8), ("OM", 5), ("P", 1, 0, 0), ("P", 1, 0, 1),
+    ("Q", 0, 1, 0), ("plane", 2, 2), ("mx", 0), ("P", 1, 0, 2), ("O", 7), ("OM", 6), ("EM", 6), ("inv", 1, 0),
+    ("X", 0, 1, 0, 3), ("E", 7), ("F", 6), ("issue", 9), ("FM", 4), ("X", 0, 1, 3, 4), ("P", 1, 1, 2),
+    ("Q", 1, 0, 0), ("P", 1, 1, 1), ("EM", 7), ("P", 1, 1, 0), ("O", 8), ("M", 7), ("Q", 1, 0, 1), ("plane", 3, 1),
+    ("plane", 3, 0), ("E", 8), ("F", 7), ("FM", 5), ("issue", 10), ("Q", 1, 0, 2), ("plane", 2, 3), ("P", 1, 1, 3),
+    ("inv", 1, 1), ("P", 1, 0, 3), ("M", 8), ("EM", 8), ("O", 9), ("Q", 1, 1, 2), ("E", 9), ("OM", 7), ("F", 8),
+    ("issue", 11), ("O", 10), ("plane", 3, 2), ("Q", 1, 1, 1), ("EM", 9), ("FM", 6), ("plane", 4, 1), ("E", 10),
+    ("OM", 8), ("EM", 10), ("Q", 1, 1, 0), ("M", 9), ("E", 11), ("F", 9), ("issue", 12), ("plane", 4, 0), ("EM", 11),
+    ("O", 11), ("FM", 7), ("Q", 1, 1, 3), ("mx", 1), ("E", 12), ("F", 10), ("M", 10), ("issue", 13), ("plane", 3, 3),
+    ("X", 1, 1, 0, 2), ("EM", 12), ("X", 1, 1, 2, 3), ("Q", 1, 0, 3), ("X", 1, 1, 3, 4), ("FM", 8), ("E", 13),
+    ("OM", 9), ("P", 2, 1, 0), ("P", 2, 1, 1), ("M", 11), ("EM", 13), ("F", 11), ("X", 1, 0, 0, 1), ("plane", 4, 2),
+    ("X", 1, 0, 1, 2), ("O", 12), ("P", 2, 1, 2), ("inv", 2, 1), ("F", 12), ("X", 1, 0, 2, 3), ("OM", 10), ("FM", 9),
+    ("X", 1, 0, 3, 4), ("P", 2, 0, 1), ("M", 12), ("O", 13), ("plane", 4, 3), ("P", 2, 1, 3), ("P", 2, 0, 3),
+    ("F", 13), ("P", 2, 0, 0), ("OM", 11), ("FM", 10), ("H", 0), ("inv", 2, 0), ("P", 2, 0, 2), ("M", 13),
+    ("bplane", 10), ("FM", 11), ("Q", 2, 0, 1), ("OM", 12), ("bplane", 11), ("FM", 12), ("OM", 13), ("H", 1),
+    ("bplane", 12), ("FM", 13), ("bplane", 13), ("Q", 2, 0, 3), ("Q", 2, 0, 0), ("Q", 2, 0, 2), ("X", 2, 0, 0, 4),
+]
+END_ORDER = [
+    ("ey", 0), ("eown", 0), ("eM", 0), ("st", 0), ("ey", 1), ("eown", 1), ("eM", 1), ("st", 1), ("st", 2), ("ey", 2),
+    ("ey", 3), ("eown", 2), ("ey", 4), ("eM", 2), ("eown", 3), ("ey", 5), ("eI", 2), ("eM", 3), ("st", 3),
+    ("eown", 4), ("ey", 6), ("eM", 4), ("eown", 5), ("ey", 7), ("eM", 5), ("eown", 6), ("ey", 8), ("eO", 2),
+    ("eIM", 2), ("eM", 6), ("eown", 7), ("ey", 9), ("eI", 3), ("eM", 7), ("eown", 8), ("ey", 10), ("eM", 8),
+    ("eown", 9), ("ey", 11), ("eOM", 2), ("eO", 3), ("eM", 9), ("eown", 10), ("ey", 12), ("eIM", 3), ("eM", 10),
+    ("eown", 11), ("ey", 13), ("eM", 11), ("eown", 12), ("eF", 2), ("eOM", 3), ("eM", 12), ("eown", 13), ("eF", 3),
+    ("eM", 13), ("eI", 6), ("eFM", 2), ("epl", 2), ("eFM", 3), ("eO", 6), ("epl", 3), ("eIM", 6), ("eI", 7),
+    ("eOM", 6), ("eIM", 7), ("emx", 0, 0), ("emx", 0, 1), ("emy", 0, 0), ("eO", 7), ("emy", 0, 1), ("eX", 0, 0, 2),
+    ("eF", 6), ("eX", 0, 2, 4), ("eOM", 7), ("eF", 7), ("eI", 10), ("eFM", 6), ("eI", 11), ("epl", 6), ("eO", 10),
+    ("eFM", 7), ("epl", 7), ("eIM", 10), ("eIM", 11), ("eI", 12), ("eOM", 10), ("eO", 11), ("eIM", 12),
+    ("emx", 1, 0), ("eOM", 11), ("emx", 1, 1), ("eF", 10), ("emy", 1, 0), ("eI", 13), ("eF", 11), ("emy", 1, 1),
+    ("eX", 1, 0, 1), ("eFM", 10), ("eX", 1, 1, 2), ("eO", 12), ("eX", 1, 2, 3), ("eIM", 13), ("epl", 10),
+    ("eX", 1, 3, 4), ("eF", 12), ("eFM", 11), ("eO", 13), ("epl", 11), ("eOM", 12), ("eF", 13), ("eFM", 12),
+    ("epl", 12), ("eOM", 13), ("emx", 2, 0), ("eFM", 13), ("epl", 13), ("emx", 2, 1), ("emy", 2, 0), ("emy", 2, 1),
+    ("eX", 2, 0, 4),
+]
+
+
+def phase_table(feats):
     table = []
-    for layer in range(layers):
-        table.append((2 * layer, 0, feats))
-        count = PIECES if layer == layers - 1 else 1
+    for buf, count in enumerate(PIECES):
         width = feats // count
-        table += [(2 * layer + 1, k * width, width) for k in range(count)]
+        table += [(buf, k * width, width) for k in range(count)]
     return table
 
 
 def kernel(
     n_z, layers, halo,
     x_ref, gain_ref, wi_ref, scale_ref, wo_ref, o_ref,
-    held, state, xg, edge, p_send, p_recv, mix, stage, part_sq, inv_col, sq_send, sq_recv,
-    w_send, w_recv, local_sem, e_send, e_recv, s_send, s_recv, a_send, a_recv, f_send, f_recv,
+    held, state, xg, edge, p_send, p_recv, mix, mix_in, part_sq, inv_col, sq_send, sq_recv,
+    w_send, w_recv, local_sem, e_send, e_recv, s_send, s_recv, a_send, a_recv, m_send, m_recv,
 ):
     rows, feats = x_ref.shape
     total = rows + halo
@@ -88,9 +132,11 @@
     pools = scale_ref.shape[1]
     chunk = pools // n_z
     last = layers - 1
-    table = phase_table(layers, feats)
+    table = phase_table(feats)
     phases = len(table)
     lanes = 128
+    quarter = feats // 4
+    state_chunks = s_send.shape[0]
     sq_tiles = part_sq.shape[1] // lanes
     s = lax.axis_index("sp")
     t = lax.axis_index("tp")
@@ -127,13 +173,24 @@
 
     sent = []
 
-    def send(src, dst, send_sem, recv_sem, to):
+    def send(src, dst, send_sem, recv_sem, to, when=None):
         copy = pltpu.make_async_remote_copy(
             src_ref=src, dst_ref=dst, send_sem=send_sem, recv_sem=recv_sem,
             device_id=to, device_id_type=MESH_ID,
         )
-        copy.start()
-        sent.append(copy)
+        if when is None:
+            copy.start()
+        else:
+            pl.when(when)(copy.start)
+        sent.append((copy, when))
+
+    def drain():
+        for copy, when in sent:
+            if when is None:
+                copy.wait_send()
+            else:
+                pl.when(when)(copy.wait_send)
+        sent.clear()
 
     def arrived(ref, sem):
         pltpu.make_async_remote_copy(
@@ -169,8 +226,23 @@
     def wait_block(ph, block, piece=whole):
         arrived(slot(ph, block, piece), recv_sem(ph, block, piece))
 
-    state_rows = rows // STATE_CHUNKS
-    final_cols = feats // PIECES
+    state_rows = rows // state_chunks
+    locals_ = {}
+
+    def parts_of(buf):
+        return [ph for ph in range(phases) if table[ph][0] == buf]
+
+    def is_out(ph):
+        return table[ph][0] % 2 == 1
+
+    def keep_own(ph):
+        copy = pltpu.make_async_copy(own(ph), slot(ph, s), local_sem.at[ph])
+        copy.start()
+        locals_[ph] = copy
+
+    def from_core_mate(ph, zz):
+        for yy in range(2):
+            wait_block(ph, block_of(zz, yy, 1 - core))
 
     def send_edge():
         send(
@@ -178,71 +250,141 @@
             e_send.at[0], e_recv.at[after_slot], after_holder,
         )
 
+    def run(table_of_steps, order):
+        for name, *args in order:
+            with jax.named_scope("_".join([name] + [str(a) for a in args])):
+                table_of_steps[name](*args)
+
     def end_program():
-        greet([inner, y_mate])
-        pl.semaphore_wait(barrier, 3)
-        mate = block_of(z, 1 - y, core)
-
-        def ship(k):
+        greet([inner, y_mate, c_mate, x_mate])
+        pl.semaphore_wait(barrier, 5)
+        send_edge()
+        mate = block_of(z_end, 1 - y, core)
+        columns = [z_in, z_over, z_far]
+
+        def own_aside(ph):
+            if is_out(ph) or not EDGE_BY_MATE[table[ph][0]]:
+                send_own(ph, y_mate)
+            if is_out(ph):
+                send_own(ph, c_mate)
+                keep_own(ph)
+
+        def own_inward(ph):
+            send_own(ph, inner)
+
+        def mate_inward(ph):
+            direct = not EDGE_BY_MATE[table[ph][0]]
+            if is_out(ph) or direct:
+                wait_block(ph, mate)
+            if direct:
+                forward(ph, mate, inner)
+            if is_out(ph):
+                forward(ph, mate, c_mate)
+
+        def ship_state(k):
             at = pl.ds(k * state_rows, state_rows)
             send(
                 x_ref.at[at], state.at[1, pl.ds(halo + k * state_rows, state_rows)],
                 s_send.at[k], s_recv.at[k], inner,
             )
 
-        send_own(0, y_mate)
-        send_own(0, inner)
-        send_edge()
-        send_own(1, y_mate)
-        wait_block(0, mate)
-        forward(0, mate, inner)
-        for k in range(STATE_CHUNKS):
-            ship(k)
-        for ph in range(1, phases):
-            send_own(ph, inner)
-            if ph + 1 < phases:
-                send_own(ph + 1, y_mate)
-            wait_block(ph, mate)
-            forward(ph, mate, inner)
-        for k in range(PIECES):
-            at = pl.ds(k * final_cols, final_cols)
-            arrived(o_ref.at[:, at], f_recv.at[k])
-        for copy in sent:
-            copy.wait_send()
-        sent.clear()
+        def take_column(which, ph):
+            block = block_of(columns[which], y, core)
+            wait_block(ph, block)
+            forward(ph, block, y_mate)
+            forward(ph, block, c_mate)
+
+        def take_mate_column(which, ph):
+            block = block_of(columns[which], 1 - y, core)
+            wait_block(ph, block)
+            forward(ph, block, c_mate)
+
+        def gathered(ph):
+            locals_[ph].wait()
+            for zz in range(n_z):
+                from_core_mate(ph, zz)
+
+        def take_mix(layer, j):
+            zz = 2 * t + j
+            ref, sem = mix_in.at[layer, zz], m_recv.at[layer, zz]
+            arrived(ref, sem)
+            send(ref, ref, m_send.at[layer, j], sem, x_mate)
+
+        def take_mate_mix(layer, j):
+            zz = 2 * (1 - t) + j
+            arrived(mix_in.at[layer, zz], m_recv.at[layer, zz])
+
+        def end_expand(layer, begin, end):
+            width = 256
+            at = pl.ds(halo, rows)
+
+            @pl.loop(begin * quarter // width, end * quarter // width)
+            def _(n):
+                cols = pl.ds(pl.multiple_of(n * width, width), width)
+                mixed = jnp.concatenate([mix_in[layer, c] for c in range(n_z)], axis=1)
+                weight = held[2 * layer + 1, :, :, cols].reshape(pools, width)
+                branch = jnp.dot(mixed, weight, preferred_element_type=jnp.float32)
+                old = x_ref[:, cols] if layer == 0 else state[1, at, cols]
+                new = (old.astype(jnp.float32) + branch).astype(jnp.bfloat16)
+                if layer == last:
+                    o_ref[:, cols] = new
+                else:
+                    state[1, at, cols] = new
+
+        part = functools.partial
+        run({
+            "ey": own_aside, "eown": own_inward, "eM": mate_inward, "st": ship_state,
+            "eI": part(take_column, 0), "eO": part(take_column, 1), "eF": part(take_column, 2),
+            "eIM": part(take_mate_column, 0), "eOM": part(take_mate_column, 1),
+            "eFM": part(take_mate_column, 2), "epl": gathered,
+            "emx": take_mix, "emy": take_mate_mix, "eX": end_expand,
+        }, END_ORDER)
+        drain()
 
     def inner_program():
         greet([opposite, y_mate, c_mate, x_mate, outer] + before)
         pl.semaphore_wait(barrier, 6)
-        locals_ = {}
+        send_edge()
         chunk_z = [z_in, z_end, z_over, z_far]
 
         def issue(ph):
-            if ph >= phases:
-                return
             send_own(ph, opposite)
             send_own(ph, y_mate)
             send_own(ph, c_mate)
-            copy = pltpu.make_async_copy(own(ph), slot(ph, s), local_sem.at[ph])
-            copy.start()
-            locals_[ph] = copy
+            if is_out(ph):
+                send_own(ph, outer)
+            keep_own(ph)
+
+        def over_pieces(ph):
+            share = OVER_BY_MATE[table[ph][0]]
+            by_mate = None if share == 0 else whole if share == 1 else first
+            direct = None if share == 1 else whole if share == 0 else second
+            return by_mate, direct
 
         def take_end(ph):
             block = block_of(z_end, y, core)
             wait_block(ph, block)
             forward(ph, block, opposite)
+            if EDGE_BY_MATE[table[ph][0]]:
+                forward(ph, block, y_mate)
             forward(ph, block, c_mate)
 
         def take_over(ph):
             block = block_of(z_over, y, core)
             wait_block(ph, block)
-            forward(ph, block, y_mate, first)
-            forward(ph, block, c_mate)
+            by_mate, _ = over_pieces(ph)
+            if by_mate is not None:
+                forward(ph, block, y_mate, by_mate)
+            forward(ph, block, c_mate)
+            if is_out(ph):
+                forward(ph, block, outer)
 
         def take_mate(ph):
             block = block_of(z_in, 1 - y, core)
             wait_block(ph, block)
-            forward(ph, block, opposite, second)
+            _, direct = over_pieces(ph)
+            if direct is not None:
+                forward(ph, block, opposite, direct)
             forward(ph, block, c_mate)
 
         def take_far(ph):
@@ -250,6 +392,8 @@
             wait_block(ph, block)
             forward(ph, block, y_mate)
             forward(ph, block, c_mate)
+            if is_out(ph):
+                forward(ph, block, outer)
 
         def take_mate_end(ph):
             block = block_of(z_end, 1 - y, core)
@@ -258,8 +402,9 @@
 
         def take_mate_over(ph):
             block = block_of(z_over, 1 - y, core)
-            wait_block(ph, block, first)
-            wait_block(ph, block, second)
+            for piece in over_pieces(ph):
+                if piece is not None:
+                    wait_block(ph, block, piece)
             forward(ph, block, c_mate)
 
         def take_mate_far(ph):
@@ -270,8 +415,15 @@
         def plane(ph, k):
             if k == 0:
                 locals_[ph].wait()
-            for yy in range(2):
-                wait_block(ph, block_of(chunk_z[k], yy, 1 - core))
+            from_core_mate(ph, chunk_z[k])
+
+        def planes_of(buf, k):
+            for ph in parts_of(buf):
+                plane(ph, k)
+
+        def all_planes(ph):
+            for k in range(n_z):
+                plane(ph, k)
 
         def first_row(layer):
             return REACH * layer
@@ -290,8 +442,14 @@
                 sq_send[layer, g, k] = jnp.broadcast_to(value, (8, lanes))
             exchange(sq_send.at[layer, g], sq_recv.at[layer, g], layer, g, n_z)
 
-        def exchange(src, dst, layer, g, k):
-            send(src, dst, a_send.at[layer, g, k], a_recv.at[layer, g, k], x_mate)
+        def exchange(src, dst, layer, g, k, when=None):
+            send(src, dst, a_send.at[layer, g, k], a_recv.at[layer, g, k], x_mate, when)
+
+        def halved(layer, g):
+            return layer == last and g == 1
+
+        def mix_slot(layer, g):
+            return 0 if g == 0 else 1 + layer
 
         def take_edge(g):
             arrived(edge.at[g], e_recv.at[g])
@@ -324,13 +482,15 @@
 
         def project(layer, g, k):
             at = from_row(first_row(layer))
-            weight = held[2 * layer, pl.ds(chunk_z[k] * 4, 4)].reshape(chunk, feats)
+            zz = chunk_z[k]
+            weight = held[2 * layer, pl.ds(zz * 4, 4)].reshape(chunk, feats)
             value = lax.dot_general(
                 xg[g, at], weight, (((1,), (1,)), ((), ())),
                 preferred_element_type=jnp.float32,
             )
-            p_send[layer, g, k, at] = value.astype(jnp.bfloat16)
-            exchange(p_send.at[layer, g, k, at], p_recv.at[layer, g, k, at], layer, g, k)
+            p_send[layer, g, zz, at] = value.astype(jnp.bfloat16)
+            when = (zz // 2 != t) if halved(layer, g) else None
+            exchange(p_send.at[layer, g, zz, at], p_recv.at[layer, g, zz, at], layer, g, zz, when)
 
         def inverse(layer, g):
             arrived(sq_recv.at[layer, g], a_recv.at[layer, g, n_z])
@@ -340,10 +500,27 @@
                 inv_col[g, pl.ds(k * lanes, lanes)] = jnp.broadcast_to(inv[0:1], (lanes, lanes)).T
 
         def pool(layer, g, k):
+            pool_plane(layer, g, chunk_z[k])
+
+        def pool_half(j):
+            pool_plane(last, 1, 2 * t + j)
+            ship_mix(last, j)
+
+        def ship_mix(layer, j):
+            zz = 2 * t + j
+            send(
+                mix.at[mix_slot(layer, 1), zz, pl.ds(halo, rows)], mix_in.at[layer, zz],
+                m_send.at[layer, j], m_recv.at[layer, zz], outer,
+            )
+
+        def ship_mixes(layer):
+            for j in range(2):
+                ship_mix(layer, j)
+
+        def pool_plane(layer, g, group):
             start = first_row(layer)
             at = from_row(start)
-            arrived(p_recv.at[layer, g, k, at], a_recv.at[layer, g, k])
-            group = chunk_z[k]
+            arrived(p_recv.at[layer, g, group, at], a_recv.at[layer, g, group])
             row = lax.broadcasted_iota(jnp.int32, (total - start, lanes), 0)
             position = (s_in if g == 0 else s_end) * rows - halo + start + row
             span = jnp.left_shift(jnp.int32(2), group)
@@ -352,8 +529,8 @@
             inv = inv_col[g, at]
             for j in range(chunk // lanes):
                 cols = pl.ds(j * lanes, lanes)
-                joined = p_send[layer, g, k, at, cols].astype(jnp.float32)
-                joined = joined + p_recv[layer, g, k, at, cols].astype(jnp.float32)
+                joined = p_send[layer, g, group, at, cols].astype(jnp.float32)
+                joined = joined + p_recv[layer, g, group, at, cols].astype(jnp.float32)
                 base = (joined * inv).astype(jnp.bfloat16).astype(jnp.float32)
                 running = base
                 width = 1
@@ -364,26 +541,25 @@
                     picked = running if picked is None else jnp.where(group >= step, running, picked)
                 lane = pl.multiple_of(group * chunk + j * lanes, lanes)
                 scale = scale_ref[pl.ds(layer, 1), pl.ds(lane, lanes)]
-                mix[g, group, at, cols] = ((picked * share - base) * scale).astype(jnp.bfloat16)
-
-        def expand(layer, g, start, stop):
+                mix[mix_slot(layer, g), group, at, cols] = ((picked * share - base) * scale).astype(jnp.bfloat16)
+
+        def expand(layer, g, begin, end):
             width = 256
             at = from_row(first_row(layer + 1))
             buf = 2 * layer + 1
-
-            @pl.loop(start // width, stop // width)
+            if layer < last and begin == 0:
+                part_sq[g] = jnp.zeros(part_sq.shape[1:], jnp.float32)
+
+            @pl.loop(begin * quarter // width, end * quarter // width)
             def _(n):
                 col = pl.multiple_of(n * width, width)
                 cols = pl.ds(col, width)
-                mixed = jnp.concatenate([mix[g, c, at] for c in range(n_z)], axis=1)
+                mixed = jnp.concatenate([mix[mix_slot(layer, g), c, at] for c in range(n_z)], axis=1)
                 weight = held[buf, :, :, cols].reshape(pools, width)
                 branch = jnp.dot(mixed, weight, preferred_element_type=jnp.float32)
                 new = (state[g, at, cols].astype(jnp.float32) + branch).astype(jnp.bfloat16)
                 if layer == last:
-                    if g == 0:
-                        o_ref[:, cols] = new
-                    else:
-                        stage[:, cols] = new
+                    o_ref[:, cols] = new
                 else:
                     state[g, at, cols] = new
                     wide = new.astype(jnp.float32)
@@ -394,173 +570,36 @@
                         sums = sums + square[:, j * lanes:(j + 1) * lanes]
                     part_sq[g, at] = part_sq[g, at] + sums
 
-        def clear(g):
-            part_sq[g] = jnp.zeros(part_sq.shape[1:], jnp.float32)
-
-        def return_final(k):
-            cols = pl.ds(k * final_cols, final_cols)
-            send(stage.at[:, cols], o_ref.at[:, cols], f_send.at[k], f_recv.at[k], outer)
-
-        def early(ph):
-            take_end(ph)
-            take_over(ph)
-            take_mate(ph)
-
-        def middle(ph):
-            take_far(ph)
-            take_mate_end(ph)
-
-        def late(ph):
-            take_mate_over(ph)
-            take_mate_far(ph)
-
-        def planes(ph):
-            for k in range(n_z):
-                plane(ph, k)
-
-        a_of = [i for i, row in enumerate(table) if row[0] % 2 == 0]
-        b_of = [[i for i, row in enumerate(table) if row[0] == 2 * l + 1] for l in range(layers)]
-
-        send_edge()
-        issue(0)
-        issue(1)
-        clear(0)
-        clear(1)
-        own_state()
-        take_edge(0)
-        squares(0, 0, total)
-        pack_squares(0, 0)
-        early(0)
-        plane(0, 0)
-        project(0, 0, 0)
-        middle(0)
-        plane(0, 1)
-        project(0, 0, 1)
-        issue(2)
-        early(1)
-        late(0)
-        plane(0, 2)
-        project(0, 0, 2)
-        plane(0, 3)
-        project(0, 0, 3)
-        inverse(0, 0)
-        pool(0, 0, 0)
-        take_edge(1)
-        squares(1, 0, halo)
-        middle(1)
-        for k in range(2):
+            if layer < last and end == 4:
+                pack_squares(g, layer + 1)
+
+        def prepare():
+            for g in range(2):
+                part_sq[g] = jnp.zeros(part_sq.shape[1:], jnp.float32)
+            own_state()
+
+        def first_squares(g):
+            take_edge(g)
+            squares(g, 0, total if g == 0 else halo)
+            pack_squares(g, 0)
+
+        def shipped_squares(k):
             take_state(k)
             squares(1, halo + k * state_rows, halo + (k + 1) * state_rows)
-        pool(0, 0, 1)
-        issue(3)
-        late(1)
-        pool(0, 0, 2)
-        for k in range(2, STATE_CHUNKS):
-            take_state(k)
-            squares(1, halo + k * state_rows, halo + (k + 1) * state_rows)
-        pack_squares(1, 0)
-        project(0, 1, 0)
-        project(0, 1, 1)
-        early(2)
-        project(0, 1, 2)
-        project(0, 1, 3)
-        pool(0, 0, 3)
-        clear(0)
-        planes(1)
-        expand(0, 0, 0, feats)
-        pack_squares(0, 1)
-        middle(2)
-        issue(4)
-        plane(2, 0)
-        project(1, 0, 0)
-        plane(2, 1)
-        project(1, 0, 1)
-        early(3)
-        late(2)
-        plane(2, 2)
-        project(1, 0, 2)
-        inverse(0, 1)
-        pool(0, 1, 0)
-        plane(2, 3)
-        project(1, 0, 3)
-        for k in range(1, n_z):
-            pool(0, 1, k)
-        clear(1)
-        middle(3)
-        expand(0, 1, 0, feats)
-        pack_squares(1, 1)
-        issue(5)
-        for k in range(n_z):
-            project(1, 1, k)
-        late(3)
-        early(4)
-        inverse(1, 0)
-        for k in range(n_z):
-            pool(1, 0, k)
-        planes(3)
-        clear(0)
-        middle(4)
-        issue(6)
-        expand(1, 0, 0, feats)
-        pack_squares(0, 2)
-        plane(4, 0)
-        project(2, 0, 0)
-        plane(4, 1)
-        project(2, 0, 1)
-        early(5)
-        inverse(1, 1)
-        for k in range(n_z):
-            pool(1, 1, k)
-        clear(1)
-        expand(1, 1, 0, feats)
-        pack_squares(1, 2)
-        project(2, 1, 0)
-        project(2, 1, 1)
-        late(4)
-        plane(4, 2)
-        project(2, 0, 2)
-        project(2, 1, 2)
-        plane(4, 3)
-        project(2, 1, 3)
-        project(2, 0, 3)
-        middle(5)
-        issue(7)
-        early(6)
-        inverse(2, 1)
-        pool(2, 1, 0)
-        late(5)
-        pool(2, 1, 1)
-        middle(6)
-        issue(8)
-        pool(2, 1, 2)
-        early(7)
-        late(6)
-        pool(2, 1, 3)
-        for piece in range(PIECES):
-            ph = b_of[last][piece]
-            planes(ph)
-            expand(last, 1, piece * final_cols, (piece + 1) * final_cols)
-            return_final(piece)
-            if piece == 0:
-                inverse(2, 0)
-                pool(2, 0, 0)
-                pool(2, 0, 1)
-                middle(7)
-                early(8)
-                late(7)
-            if piece == 1:
-                pool(2, 0, 2)
-                pool(2, 0, 3)
-                middle(8)
-                late(8)
-        expand(last, 0, 0, feats)
-        for copy in sent:
-            copy.wait_send()
-        sent.clear()
+
+        run({
+            "issue": issue, "E": take_end, "O": take_over, "M": take_mate, "F": take_far,
+            "EM": take_mate_end, "OM": take_mate_over, "FM": take_mate_far,
+            "plane": planes_of, "bplane": all_planes, "init": prepare, "sq": first_squares,
+            "st": shipped_squares, "P": project, "Q": pool, "inv": inverse, "H": pool_half,
+            "mx": ship_mixes, "X": expand,
+        }, INNER_ORDER)
+        drain()
 
     pl.when(is_end)(end_program)
     for ph in range(phases):
         count[ph] = 0
+    locals_.clear()
     pl.when(jnp.logical_not(is_end))(inner_program)
 
 
@@ -575,7 +614,8 @@
     total = rows + halo
     sq_tiles = -(-total // 128)
     chunk = pools // n_z
-    phases = len(phase_table(layers, feats))
+    phases = len(phase_table(feats))
+    state_chunks = len([row for row in END_ORDER if row[0] == "st"])
     bf, f32 = jnp.bfloat16, jnp.float32
     vmem = pl.BlockSpec(memory_space=pltpu.VMEM)
     dma = pltpu.SemaphoreType.DMA
@@ -591,23 +631,23 @@
             pltpu.VMEM((2, halo, feats), bf),
             pltpu.VMEM((layers, 2, n_z, total, chunk), bf),
             pltpu.VMEM((layers, 2, n_z, total, chunk), bf),
-            pltpu.VMEM((2, n_z, total, chunk), bf),
-            pltpu.VMEM((rows, feats), bf),
+            pltpu.VMEM((1 + layers, n_z, total, chunk), bf),
+            pltpu.VMEM((layers, n_z, rows, chunk), bf),
             pltpu.VMEM((2, sq_tiles * 128, 128), f32),
             pltpu.VMEM((2, sq_tiles * 128, 128), f32),
             pltpu.VMEM((layers, 2, sq_tiles, 8, 128), f32),
             pltpu.VMEM((layers, 2, sq_tiles, 8, 128), f32),
-            dma((phases, 14)),
+            dma((phases, 18)),
             dma((phases, blocks, 2)),
             dma((phases,)),
             dma((1,)),
             dma((2,)),
-            dma((STATE_CHUNKS,)),
-            dma((STATE_CHUNKS,)),
+            dma((state_chunks,)),
+            dma((state_chunks,)),
             dma((layers, 2, n_z + 1)),
             dma((layers, 2, n_z + 1)),
-            dma((PIECES,)),
-            dma((PIECES,)),
+            dma((layers, 2)),
+            dma((layers, n_z)),
         ],
         compiler_params=pltpu.CompilerParams(
             collective_id=0, has_side_effects=True, vmem_limit_bytes=60 * 1024 * 1024

time: 162 us -> 131 us (0.81)
  Pallas kernels: 160 us -> 127 us
    pallas_call x1, Pallas kernels: 160 us -> 127 us  [fused_body(): pl.pallas_call(functools.partial(kernel, n_z, layers, halo), out_shape=ja...]
where the time goes in v2:
time: 131 us; the launch traced here: 130 us
  Pallas kernels  127 us (97%)
  local copies, waits for them, and re-layouts  2.3 us (2%)
    pallas_call x1, Pallas kernels, fused_body(): pl.pallas_call(functools.partial(kernel, n_z, layers, halo), out_shape=ja...  127 us

profile of v2, /device:TPU:0, one launch (start us, length us, event | category | flops | bytes accessed | tf_op | source)
XLA Modules:
  0.0 129.7 jit_solution(14161144199007678291)
XLA Ops:
  0.0 127.4 %shard_map.55 = bf16[256,2048]{1,0:T(8,128)(2,1)} custom-call(bf16[256,2048]{1,0:T(8,128)(2,1)} %x_ref.1, f32[3,4096]{1,0:T(4,128)} %gain_ref.1, bf16[3,64,2048]{2,1,0:T(8,128)(2,1)} %bitcast.1, f32[3,1024]{1,0:T(4,128)} %scale_ref.1, bf16[3,64,2048]{2,1,0:T(8,128)(2,1)} %wo_ref.1), custom_call_target="tpu_custom_call" | custom-call | tf_op jit(solution)/shard_map/pallas_call | solution.py:622
  127.4 2.3 %copy.7 = bf16[256,2048]{1,0:T(8,128)(2,1)} copy(bf16[256,2048]{1,0:T(8,128)(2,1)} %shard_map.55) | data formatting | bytes 2097152

commit v3 on v2

--- a/solution.py
+++ b/solution.py
@@ -62,53 +62,48 @@
     return current
 
 
-PIECES = (2, 2, 2, 2, 2, 4)
+E, O, M, F, EM, OM1, OM2, FM = range(8)
+PIECES = (2, 2, 2, 2, 2, 2)
 EDGE_BY_MATE = (True, True, False, False, False, False)
-OVER_BY_MATE = (0.5, 0, 0.5, 1, 0, 0.5)
+OVER_BY_MATE = (0.5, 0, 0, 1, 0, 0)
 INNER_ORDER = [
-    ("init",), ("issue", 0), ("issue", 1), ("issue", 2), ("sq", 0), ("M", 0), ("O", 0), ("E", 0), ("inv", 0, 0),
-    ("O", 1), ("M", 1), ("plane", 0, 0), ("P", 0, 0, 0), ("st", 0), ("M", 2), ("O", 2), ("OM", 0), ("E", 1),
-    ("F", 0), ("EM", 0), ("issue", 3), ("Q", 0, 0, 0), ("OM", 1), ("plane", 0, 2), ("P", 0, 0, 2), ("st", 1),
-    ("EM", 1), ("OM", 2), ("plane", 0, 1), ("P", 0, 0, 1), ("FM", 0), ("F", 1), ("issue", 4), ("Q", 0, 0, 2),
-    ("st", 2), ("M", 3), ("O", 3), ("plane", 1, 0), ("Q", 0, 0, 1), ("E", 2), ("FM", 1), ("O", 4), ("plane", 0, 3),
-    ("P", 0, 0, 3), ("E", 3), ("OM", 3), ("M", 4), ("plane", 1, 2), ("EM", 2), ("F", 2), ("issue", 5),
-    ("Q", 0, 0, 3), ("st", 3), ("sq", 1), ("F", 3), ("issue", 6), ("P", 0, 1, 2), ("P", 0, 1, 1), ("EM", 3),
-    ("OM", 4), ("P", 0, 1, 3), ("E", 4), ("P", 0, 1, 0), ("plane", 1, 1), ("inv", 0, 1), ("O", 5), ("FM", 2),
-    ("EM", 4), ("Q", 0, 1, 2), ("O", 6), ("M", 5), ("E", 5), ("plane", 2, 0), ("Q", 0, 1, 1), ("FM", 3), ("F", 4),
-    ("issue", 7), ("EM", 5), ("plane", 1, 3), ("X", 0, 0, 0, 2), ("M", 6), ("plane", 2, 1), ("X", 0, 0, 2, 3),
-    ("Q", 0, 1, 3), ("X", 0, 0, 3, 4), ("E", 6), ("F", 5), ("issue", 8), ("OM", 5), ("P", 1, 0, 0), ("P", 1, 0, 1),
-    ("Q", 0, 1, 0), ("plane", 2, 2), ("mx", 0), ("P", 1, 0, 2), ("O", 7), ("OM", 6), ("EM", 6), ("inv", 1, 0),
-    ("X", 0, 1, 0, 3), ("E", 7), ("F", 6), ("issue", 9), ("FM", 4), ("X", 0, 1, 3, 4), ("P", 1, 1, 2),
-    ("Q", 1, 0, 0), ("P", 1, 1, 1), ("EM", 7), ("P", 1, 1, 0), ("O", 8), ("M", 7), ("Q", 1, 0, 1), ("plane", 3, 1),
-    ("plane", 3, 0), ("E", 8), ("F", 7), ("FM", 5), ("issue", 10), ("Q", 1, 0, 2), ("plane", 2, 3), ("P", 1, 1, 3),
-    ("inv", 1, 1), ("P", 1, 0, 3), ("M", 8), ("EM", 8), ("O", 9), ("Q", 1, 1, 2), ("E", 9), ("OM", 7), ("F", 8),
-    ("issue", 11), ("O", 10), ("plane", 3, 2), ("Q", 1, 1, 1), ("EM", 9), ("FM", 6), ("plane", 4, 1), ("E", 10),
-    ("OM", 8), ("EM", 10), ("Q", 1, 1, 0), ("M", 9), ("E", 11), ("F", 9), ("issue", 12), ("plane", 4, 0), ("EM", 11),
-    ("O", 11), ("FM", 7), ("Q", 1, 1, 3), ("mx", 1), ("E", 12), ("F", 10), ("M", 10), ("issue", 13), ("plane", 3, 3),
-    ("X", 1, 1, 0, 2), ("EM", 12), ("X", 1, 1, 2, 3), ("Q", 1, 0, 3), ("X", 1, 1, 3, 4), ("FM", 8), ("E", 13),
-    ("OM", 9), ("P", 2, 1, 0), ("P", 2, 1, 1), ("M", 11), ("EM", 13), ("F", 11), ("X", 1, 0, 0, 1), ("plane", 4, 2),
-    ("X", 1, 0, 1, 2), ("O", 12), ("P", 2, 1, 2), ("inv", 2, 1), ("F", 12), ("X", 1, 0, 2, 3), ("OM", 10), ("FM", 9),
-    ("X", 1, 0, 3, 4), ("P", 2, 0, 1), ("M", 12), ("O", 13), ("plane", 4, 3), ("P", 2, 1, 3), ("P", 2, 0, 3),
-    ("F", 13), ("P", 2, 0, 0), ("OM", 11), ("FM", 10), ("H", 0), ("inv", 2, 0), ("P", 2, 0, 2), ("M", 13),
-    ("bplane", 10), ("FM", 11), ("Q", 2, 0, 1), ("OM", 12), ("bplane", 11), ("FM", 12), ("OM", 13), ("H", 1),
-    ("bplane", 12), ("FM", 13), ("bplane", 13), ("Q", 2, 0, 3), ("Q", 2, 0, 0), ("Q", 2, 0, 2), ("X", 2, 0, 0, 4),
+    ("issue", 0), ("issue", 1), ("edge",), ("issue", 2), ("init",), ("O", 0), ("M", 0), ("E", 0), ("M", 1), ("O", 1),
+    ("plane", 0, 0), ("sq", 0), ("P", 0, 0, 0), ("O", 2), ("M", 2), ("inv", 0, 0), ("st", 0), ("OM", 0), ("F", 0),
+    ("issue", 3), ("E", 1), ("EM", 0), ("Q", 0, 0, 0), ("OM", 1), ("plane", 0, 2), ("P", 0, 0, 2), ("OM", 2),
+    ("E", 2), ("FM", 0), ("O", 3), ("M", 3), ("F", 1), ("issue", 4), ("Q", 0, 0, 2), ("st", 1), ("EM", 1),
+    ("plane", 0, 1), ("P", 0, 0, 1), ("F", 2), ("issue", 5), ("E", 3), ("EM", 2), ("OM", 3), ("FM", 1),
+    ("plane", 0, 3), ("P", 0, 0, 3), ("O", 4), ("Q", 0, 0, 1), ("st", 2), ("M", 4), ("O", 5), ("FM", 2), ("F", 3),
+    ("issue", 6), ("Q", 0, 0, 3), ("st", 3), ("sq", 1), ("P", 0, 1, 3), ("M", 5), ("P", 0, 1, 1), ("P", 0, 1, 0),
+    ("E", 4), ("OM", 4), ("plane", 2, 0), ("inv", 0, 1), ("P", 0, 1, 2), ("EM", 3), ("O", 6), ("EM", 4), ("FM", 3),
+    ("Q", 0, 1, 3), ("all", 1), ("X", 0, 0, 0, 1), ("OM", 5), ("X", 0, 0, 1, 2), ("E", 5), ("X", 0, 0, 2, 3),
+    ("M", 6), ("plane", 2, 2), ("X", 0, 0, 3, 4), ("P", 1, 0, 2), ("F", 4), ("issue", 7), ("EM", 5), ("P", 1, 0, 0),
+    ("OM", 6), ("Q", 0, 1, 1), ("plane", 2, 1), ("P", 1, 0, 1), ("F", 5), ("issue", 8), ("Q", 0, 1, 0), ("E", 6),
+    ("FM", 4), ("Q", 0, 1, 2), ("O", 7), ("inv", 1, 0), ("EM", 6), ("mx", 0), ("X", 0, 1, 0, 3), ("M", 7),
+    ("X", 0, 1, 3, 4), ("O", 8), ("E", 7), ("P", 1, 1, 1), ("P", 1, 1, 0), ("Q", 1, 0, 2), ("FM", 5), ("P", 1, 1, 2),
+    ("F", 6), ("issue", 9), ("EM", 7), ("plane", 2, 3), ("P", 1, 1, 3), ("P", 1, 0, 3), ("M", 8), ("Q", 1, 0, 0),
+    ("F", 7), ("issue", 10), ("E", 8), ("Q", 1, 0, 1), ("inv", 1, 1), ("OM", 7), ("O", 9), ("EM", 8), ("Q", 1, 1, 1),
+    ("FM", 6), ("OM", 8), ("E", 9), ("M", 9), ("Q", 1, 1, 0), ("O", 10), ("EM", 9), ("plane", 4, 0), ("plane", 4, 1),
+    ("FM", 7), ("Q", 1, 1, 2), ("F", 8), ("issue", 11), ("E", 10), ("M", 10), ("F", 9), ("Q", 1, 1, 3), ("EM", 10),
+    ("mx", 1), ("all", 3), ("X", 1, 1, 0, 3), ("FM", 8), ("X", 1, 1, 3, 4), ("E", 11), ("OM", 9), ("Q", 1, 0, 3),
+    ("P", 2, 1, 0), ("P", 2, 1, 1), ("M", 11), ("plane", 4, 2), ("P", 2, 1, 2), ("O", 11), ("inv", 2, 1), ("EM", 11),
+    ("X", 1, 0, 0, 3), ("FM", 9), ("X", 1, 0, 3, 4), ("F", 10), ("P", 2, 0, 2), ("plane", 4, 3), ("P", 2, 1, 3),
+    ("P", 2, 0, 1), ("H", 0), ("OM", 10), ("inv", 2, 0), ("P", 2, 0, 0), ("P", 2, 0, 3), ("FM", 10), ("F", 11),
+    ("Q", 2, 0, 2), ("bplane", 10), ("OM", 11), ("H", 1), ("FM", 11), ("bplane", 11), ("Q", 2, 0, 1), ("Q", 2, 0, 0),
+    ("Q", 2, 0, 3), ("X", 2, 0, 0, 4),
 ]
 END_ORDER = [
-    ("ey", 0), ("eown", 0), ("eM", 0), ("st", 0), ("ey", 1), ("eown", 1), ("eM", 1), ("st", 1), ("st", 2), ("ey", 2),
-    ("ey", 3), ("eown", 2), ("ey", 4), ("eM", 2), ("eown", 3), ("ey", 5), ("eI", 2), ("eM", 3), ("st", 3),
-    ("eown", 4), ("ey", 6), ("eM", 4), ("eown", 5), ("ey", 7), ("eM", 5), ("eown", 6), ("ey", 8), ("eO", 2),
-    ("eIM", 2), ("eM", 6), ("eown", 7), ("ey", 9), ("eI", 3), ("eM", 7), ("eown", 8), ("ey", 10), ("eM", 8),
-    ("eown", 9), ("ey", 11), ("eOM", 2), ("eO", 3), ("eM", 9), ("eown", 10), ("ey", 12), ("eIM", 3), ("eM", 10),
-    ("eown", 11), ("ey", 13), ("eM", 11), ("eown", 12), ("eF", 2), ("eOM", 3), ("eM", 12), ("eown", 13), ("eF", 3),
-    ("eM", 13), ("eI", 6), ("eFM", 2), ("epl", 2), ("eFM", 3), ("eO", 6), ("epl", 3), ("eIM", 6), ("eI", 7),
-    ("eOM", 6), ("eIM", 7), ("emx", 0, 0), ("emx", 0, 1), ("emy", 0, 0), ("eO", 7), ("emy", 0, 1), ("eX", 0, 0, 2),
-    ("eF", 6), ("eX", 0, 2, 4), ("eOM", 7), ("eF", 7), ("eI", 10), ("eFM", 6), ("eI", 11), ("epl", 6), ("eO", 10),
-    ("eFM", 7), ("epl", 7), ("eIM", 10), ("eIM", 11), ("eI", 12), ("eOM", 10), ("eO", 11), ("eIM", 12),
-    ("emx", 1, 0), ("eOM", 11), ("emx", 1, 1), ("eF", 10), ("emy", 1, 0), ("eI", 13), ("eF", 11), ("emy", 1, 1),
-    ("eX", 1, 0, 1), ("eFM", 10), ("eX", 1, 1, 2), ("eO", 12), ("eX", 1, 2, 3), ("eIM", 13), ("epl", 10),
-    ("eX", 1, 3, 4), ("eF", 12), ("eFM", 11), ("eO", 13), ("epl", 11), ("eOM", 12), ("eF", 13), ("eFM", 12),
-    ("epl", 12), ("eOM", 13), ("emx", 2, 0), ("eFM", 13), ("epl", 13), ("emx", 2, 1), ("emy", 2, 0), ("emy", 2, 1),
-    ("eX", 2, 0, 4),
+    ("ey", 0), ("ey", 1), ("eown", 0), ("eM", 0), ("edge", 1), ("st", 0), ("eown", 1), ("edge", 0), ("eM", 1),
+    ("ey", 2), ("eown", 2), ("ey", 3), ("ey", 4), ("eI", 2), ("eM", 2), ("st", 1), ("eown", 3), ("ey", 5), ("eM", 3),
+    ("st", 2), ("st", 3), ("eown", 4), ("ey", 6), ("eM", 4), ("eown", 5), ("ey", 7), ("eIM", 2), ("eO", 2),
+    ("eM", 5), ("eown", 6), ("ey", 8), ("eI", 3), ("eM", 6), ("eown", 7), ("ey", 9), ("eM", 7), ("eown", 8),
+    ("ey", 10), ("eOM", 2), ("eO", 3), ("eM", 8), ("eown", 9), ("ey", 11), ("eIM", 3), ("eF", 2), ("eM", 9),
+    ("eown", 10), ("eM", 10), ("eown", 11), ("eOM", 3), ("eM", 11), ("eF", 3), ("eFM", 2), ("eI", 6), ("eFM", 3),
+    ("eO", 6), ("eIM", 6), ("eOM", 6), ("eI", 7), ("eIM", 7), ("eO", 7), ("emx", 0, 0), ("eOM", 7), ("emx", 0, 1),
+    ("emy", 0, 0), ("eF", 6), ("emy", 0, 1), ("eall", 1), ("eX", 0, 0, 2), ("eF", 7), ("eX", 0, 2, 4), ("eFM", 6),
+    ("eI", 10), ("eFM", 7), ("eO", 10), ("eIM", 10), ("eI", 11), ("eOM", 10), ("emx", 1, 0), ("eIM", 11),
+    ("emx", 1, 1), ("emy", 1, 0), ("eO", 11), ("emy", 1, 1), ("eall", 3), ("eX", 1, 0, 2), ("eF", 10),
+    ("eX", 1, 2, 4), ("eOM", 11), ("emx", 2, 0), ("eFM", 10), ("eF", 11), ("epl", 10), ("emy", 2, 0), ("emx", 2, 1),
+    ("eFM", 11), ("epl", 11), ("emy", 2, 1), ("eX", 2, 0, 4),
 ]
 
 
@@ -124,7 +119,7 @@
     n_z, layers, halo,
     x_ref, gain_ref, wi_ref, scale_ref, wo_ref, o_ref,
     held, state, xg, edge, p_send, p_recv, mix, mix_in, part_sq, inv_col, sq_send, sq_recv,
-    w_send, w_recv, local_sem, e_send, e_recv, s_send, s_recv, a_send, a_recv, m_send, m_recv,
+    w_send, w_recv, c_recv, local_sem, e_send, e_recv, s_send, s_recv, a_send, a_recv, m_send, m_recv,
 ):
     rows, feats = x_ref.shape
     total = rows + halo
@@ -136,7 +131,8 @@
     phases = len(table)
     lanes = 128
     quarter = feats // 4
-    state_chunks = s_send.shape[0]
+    state_chunks = s_recv.shape[0]
+    last_buf = len(PIECES) - 1
     sq_tiles = part_sq.shape[1] // lanes
     s = lax.axis_index("sp")
     t = lax.axis_index("tp")
@@ -171,8 +167,6 @@
         for peer in peers:
             pl.semaphore_signal(barrier, inc=1, device_id=peer, device_id_type=MESH_ID)
 
-    sent = []
-
     def send(src, dst, send_sem, recv_sem, to, when=None):
         copy = pltpu.make_async_remote_copy(
             src_ref=src, dst_ref=dst, send_sem=send_sem, recv_sem=recv_sem,
@@ -182,15 +176,12 @@
             copy.start()
         else:
             pl.when(when)(copy.start)
-        sent.append((copy, when))
-
-    def drain():
-        for copy, when in sent:
-            if when is None:
-                copy.wait_send()
-            else:
-                pl.when(when)(copy.wait_send)
-        sent.clear()
+
+    def departed(ref, sem):
+        pltpu.make_async_remote_copy(
+            src_ref=ref, dst_ref=ref, send_sem=sem, recv_sem=sem,
+            device_id=c_mate, device_id_type=MESH_ID,
+        ).wait_send()
 
     def arrived(ref, sem):
         pltpu.make_async_remote_copy(
@@ -199,7 +190,7 @@
         ).wait_recv()
 
     whole, first, second = pl.ds(0, depth), pl.ds(0, depth // 2), pl.ds(depth // 2, depth // 2)
-    count = [0] * phases
+    volume = {}
 
     def own(ph):
         buf, start, width = table[ph]
@@ -209,46 +200,71 @@
         buf, start, width = table[ph]
         return held.at[buf, block, piece, pl.ds(start, width)]
 
-    def recv_sem(ph, block, piece=whole):
-        return w_recv.at[ph, block, 1 if piece is second else 0]
-
-    def next_send(ph):
-        count[ph] += 1
-        return w_send.at[ph, count[ph] - 1]
-
-    def send_own(ph, to):
-        send(own(ph), slot(ph, s), next_send(ph), recv_sem(ph, s), to)
-
-    def forward(ph, block, to, piece=whole):
+    def send_sem(ph, port, piece):
+        buf, _, width = table[ph]
+        kind = 1 if port == EM else 0
+        share = width * (1 if piece is whole else 0.5) / feats
+        volume[buf, kind] = volume.get((buf, kind), 0) + share
+        return w_send.at[buf, kind]
+
+    def core_sem(ph, block):
+        buf, start, width = table[ph]
+        layer = buf // 2
+        if buf % 2 == 0:
+            return c_recv.at[layer * n_z + block // 4]
+        return c_recv.at[layers * n_z + layer + (start // width if buf == last_buf else 0)]
+
+    def send_own(ph, to, port):
+        sem = core_sem(ph, s) if port is None else w_recv.at[ph, port]
+        send(own(ph), slot(ph, s), send_sem(ph, port, whole), sem, to)
+
+    def forward(ph, block, to, port, piece=whole):
         ref = slot(ph, block, piece)
-        send(ref, ref, next_send(ph), recv_sem(ph, block, piece), to)
-
-    def wait_block(ph, block, piece=whole):
-        arrived(slot(ph, block, piece), recv_sem(ph, block, piece))
+        sem = core_sem(ph, block) if port is None else w_recv.at[ph, port]
+        send(ref, ref, send_sem(ph, port, piece), sem, to)
+
+    def wait_block(ph, block, port, piece=whole):
+        arrived(slot(ph, block, piece), w_recv.at[ph, port])
+
+    def drain_weights():
+        for (buf, kind), blocks_sent in volume.items():
+            assert blocks_sent == int(blocks_sent)
+            departed(held.at[buf, pl.ds(0, int(blocks_sent))], w_send.at[buf, kind])
+        volume.clear()
 
     state_rows = rows // state_chunks
-    locals_ = {}
-
     def parts_of(buf):
         return [ph for ph in range(phases) if table[ph][0] == buf]
 
     def is_out(ph):
         return table[ph][0] % 2 == 1
 
+    def local_of(ph):
+        buf, start, width = table[ph]
+        return local_sem.at[buf + (start // width if buf == last_buf else 0)]
+
     def keep_own(ph):
-        copy = pltpu.make_async_copy(own(ph), slot(ph, s), local_sem.at[ph])
-        copy.start()
-        locals_[ph] = copy
-
-    def from_core_mate(ph, zz):
-        for yy in range(2):
-            wait_block(ph, block_of(zz, yy, 1 - core))
-
-    def send_edge():
+        pltpu.make_async_copy(own(ph), slot(ph, s), local_of(ph)).start()
+
+    def gathered(buf):
+        ph = parts_of(buf)[0]
+        weight = (wi_ref if buf % 2 == 0 else wo_ref).at[buf // 2]
+        pltpu.make_async_copy(weight, held.at[buf, s], local_of(ph)).wait()
+        arrived(held.at[buf, pl.ds(0, blocks // 2)], core_sem(ph, s))
+
+    def gathered_piece(ph):
+        buf, start, width = table[ph]
+        pltpu.make_async_copy(own(ph), slot(ph, s), local_of(ph)).wait()
+        arrived(held.at[buf, pl.ds(0, blocks // 2), :, pl.ds(start, width)], core_sem(ph, s))
+
+    def send_edge(when=None):
         send(
             x_ref.at[pl.ds(rows - halo, halo)], edge.at[after_slot],
-            e_send.at[0], e_recv.at[after_slot], after_holder,
+            e_send.at[0], e_recv.at[after_slot], after_holder, when,
         )
+
+    def send_some_edges(which):
+        send_edge(after_slot == which)
 
     def run(table_of_steps, order):
         for name, *args in order:
@@ -258,57 +274,51 @@
     def end_program():
         greet([inner, y_mate, c_mate, x_mate])
         pl.semaphore_wait(barrier, 5)
-        send_edge()
         mate = block_of(z_end, 1 - y, core)
         columns = [z_in, z_over, z_far]
 
         def own_aside(ph):
             if is_out(ph) or not EDGE_BY_MATE[table[ph][0]]:
-                send_own(ph, y_mate)
+                send_own(ph, y_mate, M)
             if is_out(ph):
-                send_own(ph, c_mate)
+                send_own(ph, c_mate, None)
                 keep_own(ph)
 
         def own_inward(ph):
-            send_own(ph, inner)
+            send_own(ph, inner, E)
 
         def mate_inward(ph):
             direct = not EDGE_BY_MATE[table[ph][0]]
             if is_out(ph) or direct:
-                wait_block(ph, mate)
+                wait_block(ph, mate, M)
             if direct:
-                forward(ph, mate, inner)
+                forward(ph, mate, inner, EM)
             if is_out(ph):
-                forward(ph, mate, c_mate)
+                forward(ph, mate, c_mate, None)
 
         def ship_state(k):
             at = pl.ds(k * state_rows, state_rows)
             send(
                 x_ref.at[at], state.at[1, pl.ds(halo + k * state_rows, state_rows)],
-                s_send.at[k], s_recv.at[k], inner,
+                s_send.at[0], s_recv.at[k], inner,
             )
 
         def take_column(which, ph):
             block = block_of(columns[which], y, core)
-            wait_block(ph, block)
-            forward(ph, block, y_mate)
-            forward(ph, block, c_mate)
+            wait_block(ph, block, (E, O, F)[which])
+            forward(ph, block, y_mate, (EM, OM1, FM)[which])
+            forward(ph, block, c_mate, None)
 
         def take_mate_column(which, ph):
             block = block_of(columns[which], 1 - y, core)
-            wait_block(ph, block)
-            forward(ph, block, c_mate)
-
-        def gathered(ph):
-            locals_[ph].wait()
-            for zz in range(n_z):
-                from_core_mate(ph, zz)
+            wait_block(ph, block, (EM, OM1, FM)[which])
+            forward(ph, block, c_mate, None)
 
         def take_mix(layer, j):
             zz = 2 * t + j
             ref, sem = mix_in.at[layer, zz], m_recv.at[layer, zz]
             arrived(ref, sem)
-            send(ref, ref, m_send.at[layer, j], sem, x_mate)
+            send(ref, ref, m_send.at[layer], sem, x_mate)
 
         def take_mate_mix(layer, j):
             zz = 2 * (1 - t) + j
@@ -336,23 +346,30 @@
             "ey": own_aside, "eown": own_inward, "eM": mate_inward, "st": ship_state,
             "eI": part(take_column, 0), "eO": part(take_column, 1), "eF": part(take_column, 2),
             "eIM": part(take_mate_column, 0), "eOM": part(take_mate_column, 1),
-            "eFM": part(take_mate_column, 2), "epl": gathered,
+            "eFM": part(take_mate_column, 2), "eall": gathered, "epl": gathered_piece,
+            "edge": send_some_edges,
             "emx": take_mix, "emy": take_mate_mix, "eX": end_expand,
         }, END_ORDER)
-        drain()
+        with jax.named_scope("drain"):
+            drain_weights()
+            departed(x_ref, s_send.at[0])
+            departed(x_ref.at[pl.ds(0, halo)], e_send.at[0])
+            for layer in range(layers):
+                departed(mix_in.at[layer, pl.ds(2 * t, 2)], m_send.at[layer])
 
     def inner_program():
-        greet([opposite, y_mate, c_mate, x_mate, outer] + before)
-        pl.semaphore_wait(barrier, 6)
-        send_edge()
+        with jax.named_scope("greet"):
+            greet([opposite, y_mate, c_mate, x_mate, outer] + before)
+        with jax.named_scope("barrier"):
+            pl.semaphore_wait(barrier, 6)
         chunk_z = [z_in, z_end, z_over, z_far]
 
         def issue(ph):
-            send_own(ph, opposite)
-            send_own(ph, y_mate)
-            send_own(ph, c_mate)
+            send_own(ph, opposite, O)
+            send_own(ph, y_mate, M)
+            send_own(ph, c_mate, None)
             if is_out(ph):
-                send_own(ph, outer)
+                send_own(ph, outer, E)
             keep_own(ph)
 
         def over_pieces(ph):
@@ -363,67 +380,63 @@
 
         def take_end(ph):
             block = block_of(z_end, y, core)
-            wait_block(ph, block)
-            forward(ph, block, opposite)
+            wait_block(ph, block, E)
+            forward(ph, block, opposite, F)
             if EDGE_BY_MATE[table[ph][0]]:
-                forward(ph, block, y_mate)
-            forward(ph, block, c_mate)
+                forward(ph, block, y_mate, EM)
+            forward(ph, block, c_mate, None)
 
         def take_over(ph):
             block = block_of(z_over, y, core)
-            wait_block(ph, block)
+            wait_block(ph, block, O)
             by_mate, _ = over_pieces(ph)
             if by_mate is not None:
-                forward(ph, block, y_mate, by_mate)
-            forward(ph, block, c_mate)
+                forward(ph, block, y_mate, OM1, by_mate)
+            forward(ph, block, c_mate, None)
             if is_out(ph):
-                forward(ph, block, outer)
+                forward(ph, block, outer, O)
 
         def take_mate(ph):
             block = block_of(z_in, 1 - y, core)
-            wait_block(ph, block)
+            wait_block(ph, block, M)
             _, direct = over_pieces(ph)
             if direct is not None:
-                forward(ph, block, opposite, direct)
-            forward(ph, block, c_mate)
+                forward(ph, block, opposite, OM2, direct)
+            forward(ph, block, c_mate, None)
 
         def take_far(ph):
             block = block_of(z_far, y, core)
-            wait_block(ph, block)
-            forward(ph, block, y_mate)
-            forward(ph, block, c_mate)
+            wait_block(ph, block, F)
+            forward(ph, block, y_mate, FM)
+            forward(ph, block, c_mate, None)
             if is_out(ph):
-                forward(ph, block, outer)
+                forward(ph, block, outer, F)
 
         def take_mate_end(ph):
             block = block_of(z_end, 1 - y, core)
-            wait_block(ph, block)
-            forward(ph, block, c_mate)
+            wait_block(ph, block, EM)
+            forward(ph, block, c_mate, None)
 
         def take_mate_over(ph):
             block = block_of(z_over, 1 - y, core)
-            for piece in over_pieces(ph):
-                if piece is not None:
-                    wait_block(ph, block, piece)
-            forward(ph, block, c_mate)
+            by_mate, direct = over_pieces(ph)
+            if by_mate is not None:
+                wait_block(ph, block, OM1, by_mate)
+            if direct is not None:
+                wait_block(ph, block, OM2, direct)
+            forward(ph, block, c_mate, None)
 
         def take_mate_far(ph):
             block = block_of(z_far, 1 - y, core)
-            wait_block(ph, block)
-            forward(ph, block, c_mate)
-
-        def plane(ph, k):
+            wait_block(ph, block, FM)
+            forward(ph, block, c_mate, None)
+
+        def plane(buf, k):
             if k == 0:
-                locals_[ph].wait()
-            from_core_mate(ph, chunk_z[k])
-
-        def planes_of(buf, k):
-            for ph in parts_of(buf):
-                plane(ph, k)
-
-        def all_planes(ph):
-            for k in range(n_z):
-                plane(ph, k)
+                weight = wi_ref.at[buf // 2]
+                pltpu.make_async_copy(weight, held.at[buf, s], local_of(parts_of(buf)[0])).wait()
+            block = block_of(chunk_z[k], 0, 0)
+            arrived(held.at[buf, pl.ds(block, 2)], core_sem(parts_of(buf)[0], block))
 
         def first_row(layer):
             return REACH * layer
@@ -440,10 +453,10 @@
                 block = part_sq[g, pl.ds(k * lanes, lanes)].T
                 value = jnp.sum(block, axis=0, keepdims=True)
                 sq_send[layer, g, k] = jnp.broadcast_to(value, (8, lanes))
-            exchange(sq_send.at[layer, g], sq_recv.at[layer, g], layer, g, n_z)
-
-        def exchange(src, dst, layer, g, k, when=None):
-            send(src, dst, a_send.at[layer, g, k], a_recv.at[layer, g, k], x_mate, when)
+            send(
+                sq_send.at[layer, g], sq_recv.at[layer, g],
+                a_send.at[layer, g, 1], a_recv.at[layer, g, n_z], x_mate,
+            )
 
         def halved(layer, g):
             return layer == last and g == 1
@@ -489,8 +502,11 @@
                 preferred_element_type=jnp.float32,
             )
             p_send[layer, g, zz, at] = value.astype(jnp.bfloat16)
-            when = (zz // 2 != t) if halved(layer, g) else None
-            exchange(p_send.at[layer, g, zz, at], p_recv.at[layer, g, zz, at], layer, g, zz, when)
+            send(
+                p_send.at[layer, g, zz, at], p_recv.at[layer, g, zz, at],
+                a_send.at[layer, g, 0], a_recv.at[layer, g, zz], x_mate,
+                (zz // 2 != t) if halved(layer, g) else None,
+            )
 
         def inverse(layer, g):
             arrived(sq_recv.at[layer, g], a_recv.at[layer, g, n_z])
@@ -510,7 +526,7 @@
             zz = 2 * t + j
             send(
                 mix.at[mix_slot(layer, 1), zz, pl.ds(halo, rows)], mix_in.at[layer, zz],
-                m_send.at[layer, j], m_recv.at[layer, zz], outer,
+                m_send.at[layer], m_recv.at[layer, zz], outer,
             )
 
         def ship_mixes(layer):
@@ -590,16 +606,22 @@
         run({
             "issue": issue, "E": take_end, "O": take_over, "M": take_mate, "F": take_far,
             "EM": take_mate_end, "OM": take_mate_over, "FM": take_mate_far,
-            "plane": planes_of, "bplane": all_planes, "init": prepare, "sq": first_squares,
+            "plane": plane, "all": gathered, "bplane": gathered_piece, "edge": send_edge, "init": prepare, "sq": first_squares,
             "st": shipped_squares, "P": project, "Q": pool, "inv": inverse, "H": pool_half,
             "mx": ship_mixes, "X": expand,
         }, INNER_ORDER)
-        drain()
+        with jax.named_scope("drain"):
+            drain_weights()
+            departed(x_ref.at[pl.ds(0, halo)], e_send.at[0])
+            for layer in range(layers):
+                departed(mix_in.at[layer, pl.ds(2 * t, 2)], m_send.at[layer])
+                at = from_row(first_row(layer))
+                for g in range(2):
+                    departed(sq_send.at[layer, g], a_send.at[layer, g, 1])
+                    zz = pl.ds(2 * (1 - t), 2) if halved(layer, g) else pl.ds(0, n_z)
+                    departed(p_send.at[layer, g, zz, at], a_send.at[layer, g, 0])
 
     pl.when(is_end)(end_program)
-    for ph in range(phases):
-        count[ph] = 0
-    locals_.clear()
     pl.when(jnp.logical_not(is_end))(inner_program)
 
 
@@ -637,16 +659,17 @@
             pltpu.VMEM((2, sq_tiles * 128, 128), f32),
             pltpu.VMEM((layers, 2, sq_tiles, 8, 128), f32),
             pltpu.VMEM((layers, 2, sq_tiles, 8, 128), f32),
-            dma((phases, 18)),
-            dma((phases, blocks, 2)),
-            dma((phases,)),
+            dma((2 * layers, 2)),
+            dma((phases, 8)),
+            dma((layers * n_z + layers - 1 + PIECES[-1],)),
+            dma((2 * layers - 1 + PIECES[-1],)),
             dma((1,)),
             dma((2,)),
+            dma((1,)),
             dma((state_chunks,)),
-            dma((state_chunks,)),
+            dma((layers, 2, 2)),
             dma((layers, 2, n_z + 1)),
-            dma((layers, 2, n_z + 1)),
-            dma((layers, 2)),
+            dma((layers,)),
             dma((layers, n_z)),
         ],
         compiler_params=pltpu.CompilerParams(

time: 131 us -> 124 us (0.947)
  Pallas kernels: 127 us -> 120 us
    pallas_call x1, Pallas kernels: 127 us -> 120 us  [fused_body(): pl.pallas_call(functools.partial(kernel, n_z, layers, halo), out_shape=ja...]
where the time goes in v3:
time: 124 us; the launch traced here: 123 us
  Pallas kernels  120 us (97%)
  local copies, waits for them, and re-layouts  2.3 us (2%)
    pallas_call x1, Pallas kernels, fused_body(): pl.pallas_call(functools.partial(kernel, n_z, layers, halo), out_shape=ja...  120 us

profile of v3, /device:TPU:0, one launch (start us, length us, event | category | flops | bytes accessed | tf_op | source)
XLA Modules:
  0.0 122.5 jit_solution(8688486739103888646)
XLA Ops:
  0.0 120.2 %shard_map.55 = bf16[256,2048]{1,0:T(8,128)(2,1)} custom-call(bf16[256,2048]{1,0:T(8,128)(2,1)} %x_ref.1, f32[3,4096]{1,0:T(4,128)} %gain_ref.1, bf16[3,64,2048]{2,1,0:T(8,128)(2,1)} %bitcast.1, f32[3,1024]{1,0:T(4,128)} %scale_ref.1, bf16[3,64,2048]{2,1,0:T(8,128)(2,1)} %wo_ref.1), custom_call_target="tpu_custom_call" | custom-call | tf_op jit(solution)/shard_map/pallas_call | solution.py:644
  120.2 2.3 %copy.7 = bf16[256,2048]{1,0:T(8,128)(2,1)} copy(bf16[256,2048]{1,0:T(8,128)(2,1)} %shard_map.55) | data formatting | bytes 2097152

commit v4 on v3

--- a/solution.py
+++ b/solution.py
@@ -63,47 +63,60 @@
 
 
 E, O, M, F, EM, OM1, OM2, FM = range(8)
-PIECES = (2, 2, 2, 2, 2, 2)
+PIECES = (2, 2, 2, 4, 2, 4)
 EDGE_BY_MATE = (True, True, False, False, False, False)
-OVER_BY_MATE = (0.5, 0, 0, 1, 0, 0)
+OVER_BY_MATE = (0.5, 0.0, 0.5, 0.5, 0.5, 0.5)
 INNER_ORDER = [
-    ("issue", 0), ("issue", 1), ("edge",), ("issue", 2), ("init",), ("O", 0), ("M", 0), ("E", 0), ("M", 1), ("O", 1),
-    ("plane", 0, 0), ("sq", 0), ("P", 0, 0, 0), ("O", 2), ("M", 2), ("inv", 0, 0), ("st", 0), ("OM", 0), ("F", 0),
-    ("issue", 3), ("E", 1), ("EM", 0), ("Q", 0, 0, 0), ("OM", 1), ("plane", 0, 2), ("P", 0, 0, 2), ("OM", 2),
-    ("E", 2), ("FM", 0), ("O", 3), ("M", 3), ("F", 1), ("issue", 4), ("Q", 0, 0, 2), ("st", 1), ("EM", 1),
-    ("plane", 0, 1), ("P", 0, 0, 1), ("F", 2), ("issue", 5), ("E", 3), ("EM", 2), ("OM", 3), ("FM", 1),
-    ("plane", 0, 3), ("P", 0, 0, 3), ("O", 4), ("Q", 0, 0, 1), ("st", 2), ("M", 4), ("O", 5), ("FM", 2), ("F", 3),
-    ("issue", 6), ("Q", 0, 0, 3), ("st", 3), ("sq", 1), ("P", 0, 1, 3), ("M", 5), ("P", 0, 1, 1), ("P", 0, 1, 0),
-    ("E", 4), ("OM", 4), ("plane", 2, 0), ("inv", 0, 1), ("P", 0, 1, 2), ("EM", 3), ("O", 6), ("EM", 4), ("FM", 3),
-    ("Q", 0, 1, 3), ("all", 1), ("X", 0, 0, 0, 1), ("OM", 5), ("X", 0, 0, 1, 2), ("E", 5), ("X", 0, 0, 2, 3),
-    ("M", 6), ("plane", 2, 2), ("X", 0, 0, 3, 4), ("P", 1, 0, 2), ("F", 4), ("issue", 7), ("EM", 5), ("P", 1, 0, 0),
-    ("OM", 6), ("Q", 0, 1, 1), ("plane", 2, 1), ("P", 1, 0, 1), ("F", 5), ("issue", 8), ("Q", 0, 1, 0), ("E", 6),
-    ("FM", 4), ("Q", 0, 1, 2), ("O", 7), ("inv", 1, 0), ("EM", 6), ("mx", 0), ("X", 0, 1, 0, 3), ("M", 7),
-    ("X", 0, 1, 3, 4), ("O", 8), ("E", 7), ("P", 1, 1, 1), ("P", 1, 1, 0), ("Q", 1, 0, 2), ("FM", 5), ("P", 1, 1, 2),
-    ("F", 6), ("issue", 9), ("EM", 7), ("plane", 2, 3), ("P", 1, 1, 3), ("P", 1, 0, 3), ("M", 8), ("Q", 1, 0, 0),
-    ("F", 7), ("issue", 10), ("E", 8), ("Q", 1, 0, 1), ("inv", 1, 1), ("OM", 7), ("O", 9), ("EM", 8), ("Q", 1, 1, 1),
-    ("FM", 6), ("OM", 8), ("E", 9), ("M", 9), ("Q", 1, 1, 0), ("O", 10), ("EM", 9), ("plane", 4, 0), ("plane", 4, 1),
-    ("FM", 7), ("Q", 1, 1, 2), ("F", 8), ("issue", 11), ("E", 10), ("M", 10), ("F", 9), ("Q", 1, 1, 3), ("EM", 10),
-    ("mx", 1), ("all", 3), ("X", 1, 1, 0, 3), ("FM", 8), ("X", 1, 1, 3, 4), ("E", 11), ("OM", 9), ("Q", 1, 0, 3),
-    ("P", 2, 1, 0), ("P", 2, 1, 1), ("M", 11), ("plane", 4, 2), ("P", 2, 1, 2), ("O", 11), ("inv", 2, 1), ("EM", 11),
-    ("X", 1, 0, 0, 3), ("FM", 9), ("X", 1, 0, 3, 4), ("F", 10), ("P", 2, 0, 2), ("plane", 4, 3), ("P", 2, 1, 3),
-    ("P", 2, 0, 1), ("H", 0), ("OM", 10), ("inv", 2, 0), ("P", 2, 0, 0), ("P", 2, 0, 3), ("FM", 10), ("F", 11),
-    ("Q", 2, 0, 2), ("bplane", 10), ("OM", 11), ("H", 1), ("FM", 11), ("bplane", 11), ("Q", 2, 0, 1), ("Q", 2, 0, 0),
-    ("Q", 2, 0, 3), ("X", 2, 0, 0, 4),
+    ("init",), ("iy", 0), ("edge",), ("iy", 1), ("im", 0), ("im", 1), ("M", 0), ("E", 0), ("O", 0), ("sq", 0),
+    ("M", 1), ("O", 1), ("sqa",), ("E", 1), ("inv", 0, 0), ("EM", 0), ("OM", 0), ("F", 0), ("E", 2), ("ic", 0),
+    ("ic", 1), ("ic", 2), ("OM", 1), ("im", 2), ("plane", 0, 0), ("P", 0, 0, 0), ("plane", 0, 2), ("P", 0, 0, 2),
+    ("E", 3), ("EM", 1), ("F", 1), ("plane", 0, 1), ("P", 0, 0, 1), ("FM", 0), ("F", 2), ("Q", 0, 0, 0), ("st", 0),
+    ("im", 3), ("EM", 2), ("O", 2), ("im", 4), ("im", 5), ("iy", 2), ("iy", 3), ("iy", 4), ("iy", 5), ("ic", 3),
+    ("ic", 4), ("ic", 5), ("Q", 0, 0, 2), ("EM", 3), ("F", 3), ("im", 6), ("im", 7), ("st", 1), ("PA", 0), ("FM", 1),
+    ("PA", 2), ("O", 3), ("PA", 1), ("plane", 0, 3), ("PA", 3), ("P", 0, 0, 3), ("FM", 2), ("O", 4), ("Q", 0, 0, 1),
+    ("st", 2), ("M", 2), ("O", 5), ("O", 6), ("ic", 6), ("ic", 7), ("ic", 8), ("ic", 9), ("ic", 10), ("ic", 11),
+    ("ic", 12), ("ic", 13), ("ic", 14), ("M", 3), ("O", 7), ("st", 3), ("sq", 1), ("PB", 3), ("ic", 15), ("OM", 2),
+    ("M", 4), ("PB", 2), ("iy", 6), ("iy", 7), ("iy", 8), ("iy", 9), ("iy", 10), ("PB", 0), ("PB", 1),
+    ("Q", 0, 0, 3), ("inv", 0, 1), ("M", 5), ("OM", 3), ("Q", 0, 1, 3), ("E", 4), ("plane", 2, 0), ("Q", 0, 1, 2),
+    ("FM", 3), ("Q", 0, 1, 0), ("E", 5), ("all", 1), ("X", 0, 0, 0, 1), ("OM", 4), ("X", 0, 0, 1, 2), ("E", 6),
+    ("X", 0, 0, 2, 3), ("F", 4), ("OM", 5), ("Q", 0, 1, 1), ("X", 0, 0, 3, 4), ("E", 7), ("P", 1, 0, 0), ("E", 8),
+    ("plane", 2, 2), ("P", 1, 0, 2), ("M", 6), ("mx", 0), ("X", 0, 1, 0, 1), ("E", 9), ("F", 5), ("X", 0, 1, 1, 2),
+    ("iy", 11), ("F", 6), ("M", 7), ("im", 8), ("im", 9), ("im", 10), ("im", 11), ("inv", 1, 0), ("X", 0, 1, 2, 3),
+    ("M", 8), ("X", 0, 1, 3, 4), ("F", 7), ("P", 1, 1, 2), ("M", 9), ("E", 10), ("P", 1, 1, 0), ("F", 8),
+    ("Q", 1, 0, 0), ("OM", 6), ("E", 11), ("F", 9), ("M", 10), ("OM", 7), ("Q", 1, 0, 2), ("inv", 1, 1), ("O", 8),
+    ("EM", 4), ("FM", 4), ("O", 9), ("Q", 1, 1, 2), ("EM", 5), ("FM", 5), ("O", 10), ("plane", 2, 1), ("P", 1, 1, 1),
+    ("E", 12), ("plane", 2, 3), ("P", 1, 1, 3), ("EM", 6), ("P", 1, 0, 3), ("M", 11), ("O", 11), ("P", 1, 0, 1),
+    ("FM", 6), ("E", 13), ("Q", 1, 1, 0), ("plane", 4, 0), ("EM", 7), ("FM", 7), ("im", 12), ("im", 13), ("im", 14),
+    ("im", 15), ("EM", 8), ("Q", 1, 1, 1), ("FM", 8), ("F", 10), ("EM", 9), ("FM", 9), ("OM", 8), ("OM", 9),
+    ("Q", 1, 1, 3), ("mx", 1), ("F", 11), ("EM", 10), ("all", 3), ("X", 1, 1, 0, 2), ("OM", 10), ("X", 1, 1, 2, 4),
+    ("F", 12), ("EM", 11), ("Q", 1, 0, 3), ("P", 2, 1, 0), ("OM", 11), ("EM", 12), ("plane", 4, 1), ("P", 2, 1, 1),
+    ("F", 13), ("FM", 10), ("plane", 4, 2), ("P", 2, 1, 2), ("EM", 13), ("iy", 12), ("iy", 13), ("iy", 14),
+    ("iy", 15), ("Q", 1, 0, 1), ("X", 1, 0, 0, 1), ("O", 12), ("inv", 2, 1), ("FM", 11), ("X", 1, 0, 1, 2),
+    ("O", 13), ("X", 1, 0, 2, 3), ("FM", 12), ("plane", 4, 3), ("P", 2, 1, 3), ("O", 14), ("X", 1, 0, 3, 4),
+    ("FM", 13), ("P", 2, 0, 2), ("O", 15), ("P", 2, 0, 3), ("M", 12), ("P", 2, 0, 1), ("inv", 2, 0), ("H", 0),
+    ("M", 13), ("E", 14), ("P", 2, 0, 0), ("M", 14), ("EM", 14), ("H", 1), ("M", 15), ("E", 15), ("OM", 12),
+    ("F", 14), ("OM", 13), ("EM", 15), ("Q", 2, 0, 2), ("bplane", 12), ("OM", 14), ("bplane", 13), ("OM", 15),
+    ("F", 15), ("FM", 14), ("Q", 2, 0, 3), ("bplane", 14), ("FM", 15), ("Q", 2, 0, 1), ("bplane", 15),
+    ("Q", 2, 0, 0), ("X", 2, 0, 0, 4),
 ]
 END_ORDER = [
-    ("ey", 0), ("ey", 1), ("eown", 0), ("eM", 0), ("edge", 1), ("st", 0), ("eown", 1), ("edge", 0), ("eM", 1),
-    ("ey", 2), ("eown", 2), ("ey", 3), ("ey", 4), ("eI", 2), ("eM", 2), ("st", 1), ("eown", 3), ("ey", 5), ("eM", 3),
-    ("st", 2), ("st", 3), ("eown", 4), ("ey", 6), ("eM", 4), ("eown", 5), ("ey", 7), ("eIM", 2), ("eO", 2),
-    ("eM", 5), ("eown", 6), ("ey", 8), ("eI", 3), ("eM", 6), ("eown", 7), ("ey", 9), ("eM", 7), ("eown", 8),
-    ("ey", 10), ("eOM", 2), ("eO", 3), ("eM", 8), ("eown", 9), ("ey", 11), ("eIM", 3), ("eF", 2), ("eM", 9),
-    ("eown", 10), ("eM", 10), ("eown", 11), ("eOM", 3), ("eM", 11), ("eF", 3), ("eFM", 2), ("eI", 6), ("eFM", 3),
-    ("eO", 6), ("eIM", 6), ("eOM", 6), ("eI", 7), ("eIM", 7), ("eO", 7), ("emx", 0, 0), ("eOM", 7), ("emx", 0, 1),
-    ("emy", 0, 0), ("eF", 6), ("emy", 0, 1), ("eall", 1), ("eX", 0, 0, 2), ("eF", 7), ("eX", 0, 2, 4), ("eFM", 6),
-    ("eI", 10), ("eFM", 7), ("eO", 10), ("eIM", 10), ("eI", 11), ("eOM", 10), ("emx", 1, 0), ("eIM", 11),
-    ("emx", 1, 1), ("emy", 1, 0), ("eO", 11), ("emy", 1, 1), ("eall", 3), ("eX", 1, 0, 2), ("eF", 10),
-    ("eX", 1, 2, 4), ("eOM", 11), ("emx", 2, 0), ("eFM", 10), ("eF", 11), ("epl", 10), ("emy", 2, 0), ("emx", 2, 1),
-    ("eFM", 11), ("epl", 11), ("emy", 2, 1), ("eX", 2, 0, 4),
+    ("edge", 0), ("ey", 0), ("eown", 0), ("eM", 0), ("edge", 1), ("ey", 1), ("eown", 1), ("eM", 1), ("ey", 2),
+    ("ey", 3), ("eown", 2), ("eM", 2), ("eown", 3), ("eM", 3), ("st", 0), ("st", 1), ("st", 2), ("st", 3), ("eI", 2),
+    ("eIM", 2), ("eF", 2), ("eO", 2), ("eFM", 2), ("eI", 3), ("eOM", 2), ("eF", 3), ("eIM", 3), ("eO", 3),
+    ("eFM", 3), ("ey", 4), ("ey", 5), ("eown", 4), ("eown", 5), ("eOM", 3), ("ey", 6), ("eI", 6), ("eO", 6),
+    ("ey", 7), ("ey", 8), ("eown", 6), ("eI", 7), ("eown", 7), ("ey", 9), ("ey", 10), ("ey", 11), ("ey", 12),
+    ("eown", 8), ("eown", 9), ("eown", 10), ("eown", 11), ("ey", 13), ("ey", 14), ("ey", 15), ("eI", 8), ("eM", 4),
+    ("eI", 9), ("eI", 12), ("eM", 5), ("eown", 12), ("eI", 13), ("eM", 6), ("eI", 14), ("eown", 13), ("eIM", 6),
+    ("eO", 7), ("eOM", 6), ("eI", 15), ("eM", 7), ("eM", 8), ("eIM", 7), ("emx", 0, 0), ("eM", 9), ("emx", 0, 1),
+    ("eM", 10), ("eF", 6), ("emy", 0, 0), ("eF", 7), ("eM", 11), ("eF", 8), ("eM", 12), ("emy", 0, 1), ("eall", 1),
+    ("eX", 0, 0, 2), ("eM", 13), ("eF", 9), ("eX", 0, 2, 4), ("eO", 8), ("eO", 9), ("eIM", 8), ("eIM", 9),
+    ("eIM", 12), ("eIM", 13), ("eIM", 14), ("eOM", 7), ("eIM", 15), ("emx", 1, 0), ("eFM", 6), ("eFM", 7),
+    ("emx", 1, 1), ("eFM", 8), ("eF", 12), ("eFM", 9), ("emy", 1, 0), ("eown", 14), ("eM", 14), ("eown", 15),
+    ("eF", 13), ("eM", 15), ("eOM", 8), ("eO", 12), ("eOM", 9), ("emy", 1, 1), ("eO", 13), ("eall", 3),
+    ("eX", 1, 0, 1), ("eFM", 12), ("eX", 1, 1, 3), ("eFM", 13), ("eO", 14), ("eX", 1, 3, 4), ("eO", 15), ("eOM", 12),
+    ("epl", 12), ("eOM", 13), ("emx", 2, 0), ("epl", 13), ("eOM", 14), ("eOM", 15), ("emx", 2, 1), ("eF", 14),
+    ("emy", 2, 0), ("eF", 15), ("emy", 2, 1), ("eX", 2, 0, 1), ("eFM", 14), ("eX", 2, 1, 2), ("eFM", 15),
+    ("epl", 14), ("eX", 2, 2, 3), ("epl", 15), ("eX", 2, 3, 4),
 ]
 
 
@@ -117,10 +130,16 @@
 
 def kernel(
     n_z, layers, halo,
-    x_ref, gain_ref, wi_ref, scale_ref, wo_ref, o_ref,
-    held, state, xg, edge, p_send, p_recv, mix, mix_in, part_sq, inv_col, sq_send, sq_recv,
-    w_send, w_recv, c_recv, local_sem, e_send, e_recv, s_send, s_recv, a_send, a_recv, m_send, m_recv,
+    x_hbm, gain_ref, wi_hbm, scale_ref, wo_hbm, o_ref,
+    x_ref, wi_ref, wo_ref, held, state, xg, edge, p_send, p_recv, mix, mix_in, part_sq, inv_col, sq_send, sq_recv,
+    w_send, w_recv, c_recv, local_sem, load_sem, e_send, e_recv, s_send, s_recv, a_send, a_recv, m_send, m_recv,
 ):
+    loads = [
+        pltpu.make_async_copy(src, dst, load_sem.at[i])
+        for i, (src, dst) in enumerate([(wi_hbm, wi_ref), (x_hbm, x_ref), (wo_hbm, wo_ref)])
+    ]
+    for load in loads:
+        load.start()
     rows, feats = x_ref.shape
     total = rows + halo
     blocks, depth = held.shape[1], held.shape[2]
@@ -233,6 +252,7 @@
         volume.clear()
 
     state_rows = rows // state_chunks
+    split_row = halo + rows // 2
     def parts_of(buf):
         return [ph for ph in range(phases) if table[ph][0] == buf]
 
@@ -257,6 +277,11 @@
         pltpu.make_async_copy(own(ph), slot(ph, s), local_of(ph)).wait()
         arrived(held.at[buf, pl.ds(0, blocks // 2), :, pl.ds(start, width)], core_sem(ph, s))
 
+    def half_plane(which, j):
+        near = jnp.where(side == 0, z_in - j, z_in + j)
+        far = jnp.where(side == 0, z_over + j, z_over - j)
+        return jnp.where(which == side, near, far)
+
     def send_edge(when=None):
         send(
             x_ref.at[pl.ds(rows - halo, halo)], edge.at[after_slot],
@@ -274,6 +299,8 @@
     def end_program():
         greet([inner, y_mate, c_mate, x_mate])
         pl.semaphore_wait(barrier, 5)
+        for load in loads:
+            load.wait()
         mate = block_of(z_end, 1 - y, core)
         columns = [z_in, z_over, z_far]
 
@@ -315,13 +342,13 @@
             forward(ph, block, c_mate, None)
 
         def take_mix(layer, j):
-            zz = 2 * t + j
+            zz = half_plane(t, j)
             ref, sem = mix_in.at[layer, zz], m_recv.at[layer, zz]
             arrived(ref, sem)
             send(ref, ref, m_send.at[layer], sem, x_mate)
 
         def take_mate_mix(layer, j):
-            zz = 2 * (1 - t) + j
+            zz = half_plane(1 - t, j)
             arrived(mix_in.at[layer, zz], m_recv.at[layer, zz])
 
         def end_expand(layer, begin, end):
@@ -362,11 +389,17 @@
             greet([opposite, y_mate, c_mate, x_mate, outer] + before)
         with jax.named_scope("barrier"):
             pl.semaphore_wait(barrier, 6)
+        for load in loads:
+            load.wait()
         chunk_z = [z_in, z_end, z_over, z_far]
 
-        def issue(ph):
+        def own_across(ph):
             send_own(ph, opposite, O)
+
+        def own_to_mate(ph):
             send_own(ph, y_mate, M)
+
+        def own_near(ph):
             send_own(ph, c_mate, None)
             if is_out(ph):
                 send_own(ph, outer, E)
@@ -494,7 +527,16 @@
                 part_sq[g, at] = sums
 
         def project(layer, g, k):
-            at = from_row(first_row(layer))
+            project_rows(layer, g, k, first_row(layer), total, chunk_z[k])
+
+        def project_early(k):
+            project_rows(0, 1, k, 0, split_row, n_z + 1 + chunk_z[k])
+
+        def project_late(k):
+            project_rows(0, 1, k, split_row, total, chunk_z[k])
+
+        def project_rows(layer, g, k, start, stop, sem):
+            at = pl.ds(start, stop - start)
             zz = chunk_z[k]
             weight = held[2 * layer, pl.ds(zz * 4, 4)].reshape(chunk, feats)
             value = lax.dot_general(
@@ -504,7 +546,7 @@
             p_send[layer, g, zz, at] = value.astype(jnp.bfloat16)
             send(
                 p_send.at[layer, g, zz, at], p_recv.at[layer, g, zz, at],
-                a_send.at[layer, g, 0], a_recv.at[layer, g, zz], x_mate,
+                a_send.at[layer, g, 0], a_recv.at[layer, g, sem], x_mate,
                 (zz // 2 != t) if halved(layer, g) else None,
             )
 
@@ -519,11 +561,11 @@
             pool_plane(layer, g, chunk_z[k])
 
         def pool_half(j):
-            pool_plane(last, 1, 2 * t + j)
+            pool_plane(last, 1, half_plane(t, j))
             ship_mix(last, j)
 
         def ship_mix(layer, j):
-            zz = 2 * t + j
+            zz = half_plane(t, j)
             send(
                 mix.at[mix_slot(layer, 1), zz, pl.ds(halo, rows)], mix_in.at[layer, zz],
                 m_send.at[layer], m_recv.at[layer, zz], outer,
@@ -536,7 +578,12 @@
         def pool_plane(layer, g, group):
             start = first_row(layer)
             at = from_row(start)
-            arrived(p_recv.at[layer, g, group, at], a_recv.at[layer, g, group])
+            if layer == 0 and g == 1:
+                early, late = pl.ds(0, split_row), pl.ds(split_row, total - split_row)
+                arrived(p_recv.at[layer, g, group, early], a_recv.at[layer, g, n_z + 1 + group])
+                arrived(p_recv.at[layer, g, group, late], a_recv.at[layer, g, group])
+            else:
+                arrived(p_recv.at[layer, g, group, at], a_recv.at[layer, g, group])
             row = lax.broadcasted_iota(jnp.int32, (total - start, lanes), 0)
             position = (s_in if g == 0 else s_end) * rows - halo + start + row
             span = jnp.left_shift(jnp.int32(2), group)
@@ -595,19 +642,24 @@
             own_state()
 
         def first_squares(g):
-            take_edge(g)
-            squares(g, 0, total if g == 0 else halo)
+            if g == 0:
+                take_edge(0)
+                squares(0, 0, total)
             pack_squares(g, 0)
+
+        def halo_squares():
+            take_edge(1)
+            squares(1, 0, halo)
 
         def shipped_squares(k):
             take_state(k)
             squares(1, halo + k * state_rows, halo + (k + 1) * state_rows)
 
         run({
-            "issue": issue, "E": take_end, "O": take_over, "M": take_mate, "F": take_far,
+            "im": own_across, "iy": own_to_mate, "ic": own_near, "E": take_end, "O": take_over, "M": take_mate, "F": take_far,
             "EM": take_mate_end, "OM": take_mate_over, "FM": take_mate_far,
-            "plane": plane, "all": gathered, "bplane": gathered_piece, "edge": send_edge, "init": prepare, "sq": first_squares,
-            "st": shipped_squares, "P": project, "Q": pool, "inv": inverse, "H": pool_half,
+            "plane": plane, "all": gathered, "bplane": gathered_piece, "edge": send_edge, "init": prepare, "sq": first_squares, "sqa": halo_squares,
+            "st": shipped_squares, "P": project, "PA": project_early, "PB": project_late, "Q": pool, "inv": inverse, "H": pool_half,
             "mx": ship_mixes, "X": expand,
         }, INNER_ORDER)
         with jax.named_scope("drain"):
@@ -640,13 +692,17 @@
     state_chunks = len([row for row in END_ORDER if row[0] == "st"])
     bf, f32 = jnp.bfloat16, jnp.float32
     vmem = pl.BlockSpec(memory_space=pltpu.VMEM)
+    hbm = pl.BlockSpec(memory_space=pl.ANY)
     dma = pltpu.SemaphoreType.DMA
     return pl.pallas_call(
         functools.partial(kernel, n_z, layers, halo),
         out_shape=jax.ShapeDtypeStruct((rows, feats), bf),
-        in_specs=[vmem] * 5,
+        in_specs=[hbm, vmem, hbm, vmem, hbm],
         out_specs=vmem,
         scratch_shapes=[
+            pltpu.VMEM((rows, feats), bf),
+            pltpu.VMEM((layers, depth, feats), bf),
+            pltpu.VMEM((layers, depth, feats), bf),
             pltpu.VMEM((2 * layers, blocks, depth, feats), bf),
             pltpu.VMEM((2, total, feats), bf),
             pltpu.VMEM((2, total, feats), bf),
@@ -663,12 +719,13 @@
             dma((phases, 8)),
             dma((layers * n_z + layers - 1 + PIECES[-1],)),
             dma((2 * layers - 1 + PIECES[-1],)),
+            dma((3,)),
             dma((1,)),
             dma((2,)),
             dma((1,)),
             dma((state_chunks,)),
             dma((layers, 2, 2)),
-            dma((layers, 2, n_z + 1)),
+            dma((layers, 2, 2 * n_z + 1)),
             dma((layers,)),
             dma((layers, n_z)),
         ],

time: 124 us -> 120 us (0.968)
  Pallas kernels: 120 us -> 117 us
    pallas_call x1, Pallas kernels: 120 us -> 117 us  [fused_body(): pl.pallas_call(functools.partial(kernel, n_z, layers, halo), out_shape=ja...]
where the time goes in v4:
time: 120 us
  Pallas kernels  117 us (98%)
  local copies, waits for them, and re-layouts  2.3 us (2%)
    pallas_call x1, Pallas kernels, fused_body(): pl.pallas_call(functools.partial(kernel, n_z, layers, halo), out_shape=ja...  117 us

profile of v4, /device:TPU:0, one launch (start us, length us, event | category | flops | bytes accessed | tf_op | source)
XLA Modules:
  0.0 119.7 jit_solution(10906839684907637638)
XLA Ops:
  0.0 117.4 %shard_map.55 = bf16[256,2048]{1,0:T(8,128)(2,1)} custom-call(bf16[256,2048]{1,0:T(8,128)(2,1)} %x_hbm.1, f32[3,4096]{1,0:T(4,128)} %gain_ref.1, bf16[3,64,2048]{2,1,0:T(8,128)(2,1)} %bitcast.1, f32[3,1024]{1,0:T(4,128)} %scale_ref.1, bf16[3,64,2048]{2,1,0:T(8,128)(2,1)} %wo_hbm.1), custom_call_target="tpu_custom_call" | custom-call | tf_op jit(solution)/shard_map/pallas_call | solution.py:697
  117.4 2.3 %copy.7 = bf16[256,2048]{1,0:T(8,128)(2,1)} copy(bf16[256,2048]{1,0:T(8,128)(2,1)} %shard_map.55) | data formatting | bytes 2097152

commit v5 on v4

--- a/solution.py
+++ b/solution.py
@@ -64,59 +64,59 @@
 
 E, O, M, F, EM, OM1, OM2, FM = range(8)
 PIECES = (2, 2, 2, 4, 2, 4)
-EDGE_BY_MATE = (True, True, False, False, False, False)
-OVER_BY_MATE = (0.5, 0.0, 0.5, 0.5, 0.5, 0.5)
+EDGE_BY_MATE = (True, False, False, False, False, False)
+OVER_BY_MATE = (0.5, 0.5, 0.5, 0.5, 0.5, 0)
 INNER_ORDER = [
-    ("init",), ("iy", 0), ("edge",), ("iy", 1), ("im", 0), ("im", 1), ("M", 0), ("E", 0), ("O", 0), ("sq", 0),
-    ("M", 1), ("O", 1), ("sqa",), ("E", 1), ("inv", 0, 0), ("EM", 0), ("OM", 0), ("F", 0), ("E", 2), ("ic", 0),
-    ("ic", 1), ("ic", 2), ("OM", 1), ("im", 2), ("plane", 0, 0), ("P", 0, 0, 0), ("plane", 0, 2), ("P", 0, 0, 2),
-    ("E", 3), ("EM", 1), ("F", 1), ("plane", 0, 1), ("P", 0, 0, 1), ("FM", 0), ("F", 2), ("Q", 0, 0, 0), ("st", 0),
-    ("im", 3), ("EM", 2), ("O", 2), ("im", 4), ("im", 5), ("iy", 2), ("iy", 3), ("iy", 4), ("iy", 5), ("ic", 3),
-    ("ic", 4), ("ic", 5), ("Q", 0, 0, 2), ("EM", 3), ("F", 3), ("im", 6), ("im", 7), ("st", 1), ("PA", 0), ("FM", 1),
-    ("PA", 2), ("O", 3), ("PA", 1), ("plane", 0, 3), ("PA", 3), ("P", 0, 0, 3), ("FM", 2), ("O", 4), ("Q", 0, 0, 1),
-    ("st", 2), ("M", 2), ("O", 5), ("O", 6), ("ic", 6), ("ic", 7), ("ic", 8), ("ic", 9), ("ic", 10), ("ic", 11),
-    ("ic", 12), ("ic", 13), ("ic", 14), ("M", 3), ("O", 7), ("st", 3), ("sq", 1), ("PB", 3), ("ic", 15), ("OM", 2),
-    ("M", 4), ("PB", 2), ("iy", 6), ("iy", 7), ("iy", 8), ("iy", 9), ("iy", 10), ("PB", 0), ("PB", 1),
-    ("Q", 0, 0, 3), ("inv", 0, 1), ("M", 5), ("OM", 3), ("Q", 0, 1, 3), ("E", 4), ("plane", 2, 0), ("Q", 0, 1, 2),
-    ("FM", 3), ("Q", 0, 1, 0), ("E", 5), ("all", 1), ("X", 0, 0, 0, 1), ("OM", 4), ("X", 0, 0, 1, 2), ("E", 6),
-    ("X", 0, 0, 2, 3), ("F", 4), ("OM", 5), ("Q", 0, 1, 1), ("X", 0, 0, 3, 4), ("E", 7), ("P", 1, 0, 0), ("E", 8),
-    ("plane", 2, 2), ("P", 1, 0, 2), ("M", 6), ("mx", 0), ("X", 0, 1, 0, 1), ("E", 9), ("F", 5), ("X", 0, 1, 1, 2),
-    ("iy", 11), ("F", 6), ("M", 7), ("im", 8), ("im", 9), ("im", 10), ("im", 11), ("inv", 1, 0), ("X", 0, 1, 2, 3),
-    ("M", 8), ("X", 0, 1, 3, 4), ("F", 7), ("P", 1, 1, 2), ("M", 9), ("E", 10), ("P", 1, 1, 0), ("F", 8),
-    ("Q", 1, 0, 0), ("OM", 6), ("E", 11), ("F", 9), ("M", 10), ("OM", 7), ("Q", 1, 0, 2), ("inv", 1, 1), ("O", 8),
-    ("EM", 4), ("FM", 4), ("O", 9), ("Q", 1, 1, 2), ("EM", 5), ("FM", 5), ("O", 10), ("plane", 2, 1), ("P", 1, 1, 1),
-    ("E", 12), ("plane", 2, 3), ("P", 1, 1, 3), ("EM", 6), ("P", 1, 0, 3), ("M", 11), ("O", 11), ("P", 1, 0, 1),
-    ("FM", 6), ("E", 13), ("Q", 1, 1, 0), ("plane", 4, 0), ("EM", 7), ("FM", 7), ("im", 12), ("im", 13), ("im", 14),
-    ("im", 15), ("EM", 8), ("Q", 1, 1, 1), ("FM", 8), ("F", 10), ("EM", 9), ("FM", 9), ("OM", 8), ("OM", 9),
-    ("Q", 1, 1, 3), ("mx", 1), ("F", 11), ("EM", 10), ("all", 3), ("X", 1, 1, 0, 2), ("OM", 10), ("X", 1, 1, 2, 4),
-    ("F", 12), ("EM", 11), ("Q", 1, 0, 3), ("P", 2, 1, 0), ("OM", 11), ("EM", 12), ("plane", 4, 1), ("P", 2, 1, 1),
-    ("F", 13), ("FM", 10), ("plane", 4, 2), ("P", 2, 1, 2), ("EM", 13), ("iy", 12), ("iy", 13), ("iy", 14),
-    ("iy", 15), ("Q", 1, 0, 1), ("X", 1, 0, 0, 1), ("O", 12), ("inv", 2, 1), ("FM", 11), ("X", 1, 0, 1, 2),
-    ("O", 13), ("X", 1, 0, 2, 3), ("FM", 12), ("plane", 4, 3), ("P", 2, 1, 3), ("O", 14), ("X", 1, 0, 3, 4),
-    ("FM", 13), ("P", 2, 0, 2), ("O", 15), ("P", 2, 0, 3), ("M", 12), ("P", 2, 0, 1), ("inv", 2, 0), ("H", 0),
-    ("M", 13), ("E", 14), ("P", 2, 0, 0), ("M", 14), ("EM", 14), ("H", 1), ("M", 15), ("E", 15), ("OM", 12),
-    ("F", 14), ("OM", 13), ("EM", 15), ("Q", 2, 0, 2), ("bplane", 12), ("OM", 14), ("bplane", 13), ("OM", 15),
-    ("F", 15), ("FM", 14), ("Q", 2, 0, 3), ("bplane", 14), ("FM", 15), ("Q", 2, 0, 1), ("bplane", 15),
-    ("Q", 2, 0, 0), ("X", 2, 0, 0, 4),
+    ("im", 0), ("iy", 0), ("edge",), ("im", 1), ("im", 2), ("init",), ("iy", 1), ("iy", 2), ("ic", 0), ("ic", 1),
+    ("ic", 2), ("O", 0), ("M", 0), ("E", 0), ("O", 1), ("E", 1), ("sq", 0), ("M", 1), ("O", 2), ("E", 2),
+    ("plane", 0, 0), ("P", 0, 0, 0), ("inv", 0, 0), ("M", 2), ("OM", 0), ("E", 3), ("F", 0), ("EM", 0),
+    ("Q", 0, 0, 0), ("sqa",), ("F", 1), ("OM", 1), ("EM", 1), ("plane", 0, 2), ("P", 0, 0, 2), ("iy", 3), ("iy", 4),
+    ("iy", 5), ("plane", 0, 1), ("P", 0, 0, 1), ("F", 2), ("st", 0), ("OM", 2), ("im", 3), ("FM", 0), ("im", 4),
+    ("im", 5), ("im", 6), ("im", 7), ("im", 8), ("im", 9), ("F", 3), ("Q", 0, 0, 2), ("FM", 1), ("st", 1), ("PA", 0),
+    ("plane", 0, 3), ("PA", 3), ("O", 3), ("PA", 1), ("M", 3), ("P", 0, 0, 3), ("Q", 0, 0, 1), ("PA", 2), ("O", 4),
+    ("M", 4), ("im", 10), ("im", 11), ("st", 2), ("O", 5), ("M", 5), ("O", 6), ("ic", 3), ("ic", 4), ("ic", 5),
+    ("ic", 6), ("O", 7), ("ic", 7), ("ic", 8), ("ic", 9), ("FM", 2), ("O", 8), ("plane", 2, 0), ("st", 3), ("sq", 1),
+    ("PB", 3), ("O", 9), ("Q", 0, 0, 3), ("PB", 2), ("PB", 0), ("FM", 3), ("PB", 1), ("EM", 2), ("inv", 0, 1),
+    ("OM", 3), ("Q", 0, 1, 3), ("iy", 6), ("iy", 7), ("iy", 8), ("iy", 9), ("iy", 10), ("OM", 4), ("EM", 3),
+    ("Q", 0, 1, 2), ("O", 10), ("all", 1), ("X", 0, 0, 0, 1), ("Q", 0, 1, 0), ("X", 0, 0, 1, 2), ("E", 4),
+    ("X", 0, 0, 2, 4), ("O", 11), ("P", 1, 0, 0), ("M", 6), ("OM", 5), ("ic", 10), ("ic", 11), ("ic", 12),
+    ("Q", 0, 1, 1), ("E", 5), ("mx", 0), ("X", 0, 1, 0, 1), ("M", 7), ("X", 0, 1, 1, 2), ("im", 12), ("im", 13),
+    ("im", 14), ("plane", 2, 2), ("P", 1, 0, 2), ("F", 4), ("M", 8), ("inv", 1, 0), ("X", 0, 1, 2, 3), ("EM", 4),
+    ("OM", 6), ("X", 0, 1, 3, 4), ("M", 9), ("P", 1, 1, 2), ("Q", 1, 0, 0), ("P", 1, 1, 0), ("EM", 5), ("F", 5),
+    ("iy", 11), ("M", 10), ("OM", 7), ("E", 6), ("plane", 2, 1), ("P", 1, 1, 1), ("O", 12), ("Q", 1, 0, 2),
+    ("inv", 1, 1), ("P", 1, 0, 1), ("E", 7), ("O", 13), ("E", 8), ("O", 14), ("E", 9), ("Q", 1, 1, 2), ("OM", 8),
+    ("FM", 4), ("OM", 9), ("OM", 10), ("E", 10), ("Q", 1, 1, 0), ("FM", 5), ("F", 6), ("plane", 2, 3),
+    ("P", 1, 1, 3), ("F", 7), ("E", 11), ("P", 1, 0, 3), ("M", 11), ("Q", 1, 1, 1), ("F", 8), ("EM", 6), ("FM", 6),
+    ("plane", 4, 0), ("F", 9), ("ic", 13), ("ic", 14), ("ic", 15), ("EM", 7), ("FM", 7), ("im", 15), ("Q", 1, 0, 1),
+    ("EM", 8), ("FM", 8), ("F", 10), ("EM", 9), ("FM", 9), ("Q", 1, 1, 3), ("mx", 1), ("all", 3), ("X", 1, 1, 0, 1),
+    ("F", 11), ("X", 1, 1, 1, 2), ("EM", 10), ("X", 1, 1, 2, 3), ("OM", 11), ("X", 1, 1, 3, 4), ("FM", 10),
+    ("Q", 1, 0, 3), ("X", 1, 0, 0, 1), ("EM", 11), ("O", 15), ("plane", 4, 2), ("P", 2, 1, 0), ("P", 2, 1, 2),
+    ("E", 12), ("plane", 4, 1), ("FM", 11), ("inv", 2, 1), ("P", 2, 1, 1), ("X", 1, 0, 1, 2), ("E", 13),
+    ("plane", 4, 3), ("P", 2, 1, 3), ("X", 1, 0, 2, 3), ("EM", 12), ("X", 1, 0, 3, 4), ("F", 12), ("P", 2, 0, 2),
+    ("E", 14), ("P", 2, 0, 3), ("F", 13), ("EM", 13), ("P", 2, 0, 1), ("H", 0), ("P", 2, 0, 0), ("EM", 14),
+    ("FM", 12), ("iy", 12), ("iy", 13), ("iy", 14), ("iy", 15), ("inv", 2, 0), ("H", 1), ("F", 14), ("E", 15),
+    ("FM", 13), ("EM", 15), ("M", 12), ("Q", 2, 0, 2), ("F", 15), ("M", 13), ("M", 14), ("Q", 2, 0, 3), ("OM", 12),
+    ("M", 15), ("OM", 13), ("bplane", 12), ("FM", 14), ("bplane", 13), ("OM", 14), ("Q", 2, 0, 1), ("FM", 15),
+    ("bplane", 14), ("OM", 15), ("bplane", 15), ("Q", 2, 0, 0), ("X", 2, 0, 0, 4),
 ]
 END_ORDER = [
-    ("edge", 0), ("ey", 0), ("eown", 0), ("eM", 0), ("edge", 1), ("ey", 1), ("eown", 1), ("eM", 1), ("ey", 2),
-    ("ey", 3), ("eown", 2), ("eM", 2), ("eown", 3), ("eM", 3), ("st", 0), ("st", 1), ("st", 2), ("st", 3), ("eI", 2),
-    ("eIM", 2), ("eF", 2), ("eO", 2), ("eFM", 2), ("eI", 3), ("eOM", 2), ("eF", 3), ("eIM", 3), ("eO", 3),
-    ("eFM", 3), ("ey", 4), ("ey", 5), ("eown", 4), ("eown", 5), ("eOM", 3), ("ey", 6), ("eI", 6), ("eO", 6),
-    ("ey", 7), ("ey", 8), ("eown", 6), ("eI", 7), ("eown", 7), ("ey", 9), ("ey", 10), ("ey", 11), ("ey", 12),
-    ("eown", 8), ("eown", 9), ("eown", 10), ("eown", 11), ("ey", 13), ("ey", 14), ("ey", 15), ("eI", 8), ("eM", 4),
-    ("eI", 9), ("eI", 12), ("eM", 5), ("eown", 12), ("eI", 13), ("eM", 6), ("eI", 14), ("eown", 13), ("eIM", 6),
-    ("eO", 7), ("eOM", 6), ("eI", 15), ("eM", 7), ("eM", 8), ("eIM", 7), ("emx", 0, 0), ("eM", 9), ("emx", 0, 1),
-    ("eM", 10), ("eF", 6), ("emy", 0, 0), ("eF", 7), ("eM", 11), ("eF", 8), ("eM", 12), ("emy", 0, 1), ("eall", 1),
-    ("eX", 0, 0, 2), ("eM", 13), ("eF", 9), ("eX", 0, 2, 4), ("eO", 8), ("eO", 9), ("eIM", 8), ("eIM", 9),
-    ("eIM", 12), ("eIM", 13), ("eIM", 14), ("eOM", 7), ("eIM", 15), ("emx", 1, 0), ("eFM", 6), ("eFM", 7),
-    ("emx", 1, 1), ("eFM", 8), ("eF", 12), ("eFM", 9), ("emy", 1, 0), ("eown", 14), ("eM", 14), ("eown", 15),
-    ("eF", 13), ("eM", 15), ("eOM", 8), ("eO", 12), ("eOM", 9), ("emy", 1, 1), ("eO", 13), ("eall", 3),
-    ("eX", 1, 0, 1), ("eFM", 12), ("eX", 1, 1, 3), ("eFM", 13), ("eO", 14), ("eX", 1, 3, 4), ("eO", 15), ("eOM", 12),
-    ("epl", 12), ("eOM", 13), ("emx", 2, 0), ("epl", 13), ("eOM", 14), ("eOM", 15), ("emx", 2, 1), ("eF", 14),
-    ("emy", 2, 0), ("eF", 15), ("emy", 2, 1), ("eX", 2, 0, 1), ("eFM", 14), ("eX", 2, 1, 2), ("eFM", 15),
-    ("epl", 14), ("eX", 2, 2, 3), ("epl", 15), ("eX", 2, 3, 4),
+    ("edge", 0), ("ey", 0), ("ey", 1), ("ey", 2), ("ey", 3), ("eown", 0), ("eown", 1), ("eown", 2), ("eown", 3),
+    ("eM", 1), ("eM", 0), ("edge", 1), ("ey", 4), ("ey", 5), ("st", 0), ("st", 1), ("st", 2), ("st", 3), ("eM", 2),
+    ("eI", 2), ("eM", 3), ("eown", 4), ("eown", 5), ("eM", 4), ("eM", 5), ("eO", 2), ("eIM", 2), ("eOM", 2),
+    ("eF", 2), ("ey", 6), ("eown", 6), ("eF", 3), ("eFM", 2), ("ey", 7), ("ey", 8), ("eown", 7), ("ey", 9),
+    ("ey", 10), ("ey", 11), ("eown", 8), ("eown", 9), ("eown", 10), ("eown", 11), ("eM", 6), ("eO", 3), ("eFM", 3),
+    ("eM", 7), ("eO", 6), ("eM", 8), ("eM", 9), ("eI", 3), ("ey", 12), ("ey", 13), ("ey", 14), ("ey", 15), ("eI", 6),
+    ("eM", 10), ("eO", 7), ("eI", 7), ("eM", 11), ("eI", 8), ("eI", 9), ("eOM", 3), ("eO", 8), ("eOM", 6), ("eO", 9),
+    ("eIM", 3), ("eI", 12), ("eown", 12), ("eown", 13), ("eM", 12), ("eown", 14), ("eM", 13), ("emx", 0, 0),
+    ("eM", 14), ("eown", 15), ("eM", 15), ("emx", 0, 1), ("eIM", 6), ("emy", 0, 0), ("eO", 12), ("eOM", 7),
+    ("eO", 13), ("eIM", 7), ("emy", 0, 1), ("eall", 1), ("eX", 0, 0, 2), ("eIM", 8), ("eO", 14), ("eX", 0, 2, 4),
+    ("eIM", 9), ("eOM", 8), ("eF", 6), ("eOM", 9), ("eIM", 12), ("eF", 7), ("eOM", 12), ("eF", 8), ("eOM", 13),
+    ("eF", 9), ("eOM", 14), ("eI", 13), ("eFM", 6), ("eI", 14), ("eFM", 7), ("eI", 15), ("eFM", 8), ("eFM", 9),
+    ("emx", 1, 0), ("eIM", 13), ("eIM", 14), ("emx", 1, 1), ("eIM", 15), ("eO", 15), ("emy", 1, 0), ("eF", 12),
+    ("emy", 1, 1), ("eall", 3), ("eX", 1, 0, 1), ("eOM", 15), ("eX", 1, 1, 2), ("eF", 13), ("eX", 1, 2, 4),
+    ("eFM", 12), ("emx", 2, 0), ("epl", 12), ("eFM", 13), ("epl", 13), ("emx", 2, 1), ("eF", 14), ("emy", 2, 0),
+    ("eF", 15), ("emy", 2, 1), ("eX", 2, 0, 1), ("eFM", 14), ("eX", 2, 1, 2), ("eFM", 15), ("epl", 14),
+    ("eX", 2, 2, 3), ("epl", 15), ("eX", 2, 3, 4),
 ]
 
 
@@ -130,9 +130,9 @@
 
 def kernel(
     n_z, layers, halo,
-    x_hbm, gain_ref, wi_hbm, scale_ref, wo_hbm, o_ref,
-    x_ref, wi_ref, wo_ref, held, state, xg, edge, p_send, p_recv, mix, mix_in, part_sq, inv_col, sq_send, sq_recv,
-    w_send, w_recv, c_recv, local_sem, load_sem, e_send, e_recv, s_send, s_recv, a_send, a_recv, m_send, m_recv,
+    x_hbm, gain_ref, wi_hbm, scale_ref, wo_hbm, o_hbm,
+    x_ref, wi_ref, wo_ref, o_ref, held, state, xg, edge, p_send, p_recv, mix, mix_in, part_sq, inv_col, sq_send, sq_recv,
+    w_send, w_recv, c_recv, local_sem, load_sem, out_sem, e_send, e_recv, s_send, s_recv, a_send, a_recv, early_recv, m_send, m_recv,
 ):
     loads = [
         pltpu.make_async_copy(src, dst, load_sem.at[i])
@@ -211,6 +211,12 @@
     whole, first, second = pl.ds(0, depth), pl.ds(0, depth // 2), pl.ds(depth // 2, depth // 2)
     volume = {}
 
+    def put_out(cols):
+        pltpu.make_async_copy(o_ref.at[:, cols], o_hbm.at[:, cols], out_sem.at[0]).start()
+
+    def wait_out():
+        pltpu.make_async_copy(o_ref, o_hbm, out_sem.at[0]).wait()
+
     def own(ph):
         buf, start, width = table[ph]
         return (wi_ref if buf % 2 == 0 else wo_ref).at[buf // 2, :, pl.ds(start, width)]
@@ -365,6 +371,7 @@
                 new = (old.astype(jnp.float32) + branch).astype(jnp.bfloat16)
                 if layer == last:
                     o_ref[:, cols] = new
+                    put_out(cols)
                 else:
                     state[1, at, cols] = new
 
@@ -379,6 +386,7 @@
         }, END_ORDER)
         with jax.named_scope("drain"):
             drain_weights()
+            wait_out()
             departed(x_ref, s_send.at[0])
             departed(x_ref.at[pl.ds(0, halo)], e_send.at[0])
             for layer in range(layers):
@@ -527,13 +535,13 @@
                 part_sq[g, at] = sums
 
         def project(layer, g, k):
-            project_rows(layer, g, k, first_row(layer), total, chunk_z[k])
+            project_rows(layer, g, k, first_row(layer), total, a_recv.at[layer, g, chunk_z[k]])
 
         def project_early(k):
-            project_rows(0, 1, k, 0, split_row, n_z + 1 + chunk_z[k])
+            project_rows(0, 1, k, 0, split_row, early_recv.at[chunk_z[k]])
 
         def project_late(k):
-            project_rows(0, 1, k, split_row, total, chunk_z[k])
+            project_rows(0, 1, k, split_row, total, a_recv.at[0, 1, chunk_z[k]])
 
         def project_rows(layer, g, k, start, stop, sem):
             at = pl.ds(start, stop - start)
@@ -546,7 +554,7 @@
             p_send[layer, g, zz, at] = value.astype(jnp.bfloat16)
             send(
                 p_send.at[layer, g, zz, at], p_recv.at[layer, g, zz, at],
-                a_send.at[layer, g, 0], a_recv.at[layer, g, sem], x_mate,
+                a_send.at[layer, g, 0], sem, x_mate,
                 (zz // 2 != t) if halved(layer, g) else None,
             )
 
@@ -580,7 +588,7 @@
             at = from_row(start)
             if layer == 0 and g == 1:
                 early, late = pl.ds(0, split_row), pl.ds(split_row, total - split_row)
-                arrived(p_recv.at[layer, g, group, early], a_recv.at[layer, g, n_z + 1 + group])
+                arrived(p_recv.at[layer, g, group, early], early_recv.at[group])
                 arrived(p_recv.at[layer, g, group, late], a_recv.at[layer, g, group])
             else:
                 arrived(p_recv.at[layer, g, group, at], a_recv.at[layer, g, group])
@@ -623,6 +631,7 @@
                 new = (state[g, at, cols].astype(jnp.float32) + branch).astype(jnp.bfloat16)
                 if layer == last:
                     o_ref[:, cols] = new
+                    put_out(cols)
                 else:
                     state[g, at, cols] = new
                     wide = new.astype(jnp.float32)
@@ -664,6 +673,7 @@
         }, INNER_ORDER)
         with jax.named_scope("drain"):
             drain_weights()
+            wait_out()
             departed(x_ref.at[pl.ds(0, halo)], e_send.at[0])
             for layer in range(layers):
                 departed(mix_in.at[layer, pl.ds(2 * t, 2)], m_send.at[layer])
@@ -698,11 +708,12 @@
         functools.partial(kernel, n_z, layers, halo),
         out_shape=jax.ShapeDtypeStruct((rows, feats), bf),
         in_specs=[hbm, vmem, hbm, vmem, hbm],
-        out_specs=vmem,
+        out_specs=hbm,
         scratch_shapes=[
             pltpu.VMEM((rows, feats), bf),
             pltpu.VMEM((layers, depth, feats), bf),
             pltpu.VMEM((layers, depth, feats), bf),
+            pltpu.VMEM((rows, feats), bf),
             pltpu.VMEM((2 * layers, blocks, depth, feats), bf),
             pltpu.VMEM((2, total, feats), bf),
             pltpu.VMEM((2, total, feats), bf),
@@ -721,11 +732,13 @@
             dma((2 * layers - 1 + PIECES[-1],)),
             dma((3,)),
             dma((1,)),
+            dma((1,)),
             dma((2,)),
             dma((1,)),
             dma((state_chunks,)),
             dma((layers, 2, 2)),
-            dma((layers, 2, 2 * n_z + 1)),
+            dma((layers, 2, n_z + 1)),
+            dma((n_z,)),
             dma((layers,)),
             dma((layers, n_z)),
         ],

time: 120 us -> 116 us (0.967)
  Pallas kernels: 117 us -> 114 us
    pallas_call x1, Pallas kernels: 117 us -> 114 us  [fused_body(): pl.pallas_call(functools.partial(kernel, n_z, layers, halo), out_shape=ja...]
where the time goes in v5:
time: 116 us
  Pallas kernels  114 us (98%)
  local copies, waits for them, and re-layouts  2.3 us (2%)
    pallas_call x1, Pallas kernels, fused_body(): pl.pallas_call(functools.partial(kernel, n_z, layers, halo), out_shape=ja...  114 us

profile of v5, /device:TPU:0, one launch (start us, length us, event | category | flops | bytes accessed | tf_op | source)
XLA Modules:
  0.0 116.1 jit_solution(16782205118734615087)
XLA Ops:
  0.0 113.7 %shard_map.55 = bf16[256,2048]{1,0:T(8,128)(2,1)} custom-call(bf16[256,2048]{1,0:T(8,128)(2,1)} %x_hbm.1, f32[3,4096]{1,0:T(4,128)} %gain_ref.1, bf16[3,64,2048]{2,1,0:T(8,128)(2,1)} %bitcast.1, f32[3,1024]{1,0:T(4,128)} %scale_ref.1, bf16[3,64,2048]{2,1,0:T(8,128)(2,1)} %wo_hbm.1), custom_call_target="tpu_custom_call" | custom-call | tf_op jit(solution)/shard_map/pallas_call | solution.py:707
  113.8 2.3 %copy.7 = bf16[256,2048]{1,0:T(8,128)(2,1)} copy(bf16[256,2048]{1,0:T(8,128)(2,1)} %shard_map.55) | data formatting | bytes 2097152

commit v6 on v5

--- a/solution.py
+++ b/solution.py
@@ -358,7 +358,7 @@
             arrived(mix_in.at[layer, zz], m_recv.at[layer, zz])
 
         def end_expand(layer, begin, end):
-            width = 256
+            width = 512
             at = pl.ds(halo, rows)
 
             @pl.loop(begin * quarter // width, end * quarter // width)
@@ -615,7 +615,7 @@
                 mix[mix_slot(layer, g), group, at, cols] = ((picked * share - base) * scale).astype(jnp.bfloat16)
 
         def expand(layer, g, begin, end):
-            width = 256
+            width = 512
             at = from_row(first_row(layer + 1))
             buf = 2 * layer + 1
             if layer < last and begin == 0:

time: 116 us -> 116 us (level)
  no operation moved by 1% of the time
where the time goes in v6:
time: 116 us; the launch traced here: 115 us
  Pallas kernels  113 us (97%)
  local copies, waits for them, and re-layouts  2.3 us (2%)
    pallas_call x1, Pallas kernels, fused_body(): pl.pallas_call(functools.partial(kernel, n_z, layers, halo), out_shape=ja...  113 us

profile of v6, /device:TPU:0, one launch (start us, length us, event | category | flops | bytes accessed | tf_op | source)
XLA Modules:
  0.0 115.1 jit_solution(11594997941337503568)
XLA Ops:
  0.0 112.8 %shard_map.55 = bf16[256,2048]{1,0:T(8,128)(2,1)} custom-call(bf16[256,2048]{1,0:T(8,128)(2,1)} %x_hbm.1, f32[3,4096]{1,0:T(4,128)} %gain_ref.1, bf16[3,64,2048]{2,1,0:T(8,128)(2,1)} %bitcast.1, f32[3,1024]{1,0:T(4,128)} %scale_ref.1, bf16[3,64,2048]{2,1,0:T(8,128)(2,1)} %wo_hbm.1), custom_call_target="tpu_custom_call" | custom-call | tf_op jit(solution)/shard_map/pallas_call | solution.py:707
  112.8 2.3 %copy.7 = bf16[256,2048]{1,0:T(8,128)(2,1)} copy(bf16[256,2048]{1,0:T(8,128)(2,1)} %shard_map.55) | data formatting | bytes 2097152
